TPU v7x, 512 devices: a whole 4x4x16 slice. The times are simulated.
512 devices in a mesh: sp: 64 (over z, y), dp: 8 (over x, core).
Axes of the slice: x: 4, y: 4, z: 16, core: 2. Of those that a mesh axis runs over, the one named last changes fastest.
Arguments:
- val_input: bfloat16 [8192, 1536], P('sp', 'dp'), may hold values from -24 to 24, as said below
- gate_input: bfloat16 [8192, 1536], P('sp', 'dp'), may hold values from -8 to 8
- cotangent: bfloat16 [8192, 4096], P('sp'), may hold values from -16 to 16
- out_weight: bfloat16 [4096, 1536], P('sp', 'dp'), may hold values from -0.09375 to 0.09375
- conv_taps: float32 [31, 1536], P(None, 'dp'), may hold values from -1 to 1
- norm_gain: float32 [1536], P('dp'), may hold values from 0.1 to 1.9
Outputs:
- grad_val: bfloat16 [8192, 1536], P('sp', 'dp')
- grad_gate: bfloat16 [8192, 1536], P('sp', 'dp')
- grad_out_weight: float32 [4096, 1536], P('sp', 'dp')
- grad_taps: float32 [31, 1536], P(None, 'dp')
- grad_gain: float32 [1536], P('dp')
Inputs may be any that keep to these rules, and one draw needn't show every extreme that they name: `val_input`: blocks of 64 channels and blocks of 32 tokens carry their own scales.
All inputs are finite; a program needn't handle non-finite values.
Results may differ from a plain program's by a relative error of at most 0.0063.
Values may be sent and summed in bfloat16 or wider, within the bound.
No kernel may reach another device: no remote copies, remote signals or barrier semaphores. Data moves between devices by JAX's collectives and lax.ppermute only.
A program may use at most 64 MiB of HBM per device.

v0:
```python
import jax
import jax.numpy as jnp
from jax import lax
from jax.sharding import Mesh
from jax.sharding import PartitionSpec as P


SP = ("z_far", "z_near", "sp_1")
Z = ("z_far", "z_near")


norm_floor = 0.25


def passed_along(value, axis, steps):
    count = lax.axis_size(axis)
    first, last = (max(0, -steps), min(count, count - steps))
    return lax.ppermute(value, axis, [(source, source + steps) for source in range(first, last)])


def exchange(blocks, axis):
    return lax.all_to_all(blocks, axis, split_axis=0, concat_axis=0, tiled=True)


def from_everyone(array, axis):
    return exchange(jnp.broadcast_to(array, (lax.axis_size(axis), *array.shape)), axis)


def swapped(value, axis, k):
    return lax.ppermute(value, axis, [(i, i ^ k) for i in range(lax.axis_size(axis))])


def reordered(blocks, index):
    k = 1
    while k < len(blocks):
        swap = (index & k) != 0
        blocks = [jnp.where(swap, blocks[j ^ k], blocks[j]) for j in range(len(blocks))]
        k *= 2
    return blocks


def dense(blocks):
    half = blocks.shape[-2] // 2
    rest = jnp.concatenate([blocks[..., :half, 128:], blocks[..., half:, 128:]], -1)
    return jnp.concatenate([blocks[..., :128], rest], -2)


def undense(blocks):
    rows = blocks.shape[-2] * 2 // 3
    rest = blocks[..., rows:, :]
    rest = jnp.concatenate([rest[..., :64], rest[..., 64:]], -2)
    return jnp.concatenate([blocks[..., :rows, :], rest], -1)


def per_device(val_input, gate_input, cotangent, out_weight, conv_taps, norm_gain):
    rows_here = val_input.shape[0]
    width_dp = val_input.shape[1]
    taps = conv_taps.shape[0]
    channels = width_dp * lax.axis_size("dp")
    z_size, y_size = (lax.axis_size(Z), lax.axis_size("sp_1"))
    d_rows = out_weight.shape[0]

    y_here = lax.axis_index("sp_1")
    others = range(1, y_size)

    weight = from_everyone(dense(out_weight), Z)
    blocks = cotangent.reshape(rows_here, z_size, y_size, d_rows).transpose(2, 0, 1, 3)
    blocks = blocks.reshape(y_size, rows_here, z_size * d_rows)
    blocks = [lax.dynamic_index_in_dim(blocks, y_here ^ k, 0, False) for k in range(y_size)]
    columns = [blocks[0]] + [swapped(blocks[k], "sp_1", k) for k in others]

    sigma_gate = jax.nn.sigmoid(gate_input.astype(jnp.float32))
    mixed_in = (val_input.astype(jnp.float32) * sigma_gate).astype(jnp.bfloat16)
    earlier = passed_along(mixed_in[rows_here - (taps - 1) :], SP, 1)
    padded_in = jnp.concatenate([earlier, lax.optimization_barrier(mixed_in)], 0).astype(
        jnp.float32
    )
    conv_out = jnp.zeros((rows_here, width_dp), jnp.float32)
    for offset in range(taps):
        conv_out = conv_out + conv_taps[offset][None, :] * padded_in[offset : offset + rows_here]
    conv_rows = lax.optimization_barrier(conv_out.astype(jnp.bfloat16)).astype(jnp.float32)
    row_sums = jnp.stack([jnp.sum(conv_rows, 1), jnp.sum(conv_rows * conv_rows, 1)])
    weight, row_sums = lax.optimization_barrier((weight, row_sums))
    row_sums = from_everyone(row_sums, "dp").sum(axis=0)
    row_mean = row_sums[0][:, None] / channels
    row_var = row_sums[1][:, None] / channels - row_mean * row_mean
    inv_scale = lax.rsqrt(row_var + norm_floor)
    normed = (conv_rows - row_mean) * inv_scale
    act = normed * norm_gain[None, :]
    sigma_act = jax.nn.sigmoid(act)
    swished = (act * sigma_act).astype(jnp.bfloat16)

    weight = undense(weight).reshape(z_size * d_rows, width_dp)
    mix_parts = [
        jnp.dot(c, weight, preferred_element_type=jnp.float32).astype(jnp.bfloat16) for c in columns
    ]
    sent = [jnp.concatenate([part, swished], 1) for part in reordered(mix_parts, y_here)]
    received = exchange(jnp.stack(sent), "sp_1")
    grad_mix = received[:, :, :width_dp].astype(jnp.float32).sum(axis=0)
    swished_y = reordered([received[i, :, width_dp:] for i in range(y_size)], y_here)
    weight_part = lax.dot_general(
        jnp.concatenate(columns, 0),
        jnp.concatenate(swished_y, 0),
        (((0,), (0,)), ((), ())),
        preferred_element_type=jnp.float32,
    )
    weight_part = dense(weight_part.astype(jnp.bfloat16).reshape(z_size, d_rows, width_dp))

    grad_act = grad_mix * sigma_act * (1.0 + act * (1.0 - sigma_act))
    gain_part = jnp.sum(grad_act * normed, 0)
    grad_norm = grad_act * norm_gain[None, :]
    norm_sums = jnp.stack([jnp.sum(grad_norm, 1), jnp.sum(grad_norm * normed, 1)])
    norm_sums = from_everyone(norm_sums, "dp").sum(axis=0)
    first_sum = norm_sums[0][:, None] / channels
    second_sum = norm_sums[1][:, None] / channels
    grad_conv = (inv_scale * (grad_norm - first_sum - normed * second_sum)).astype(jnp.bfloat16)
    grad_conv = lax.optimization_barrier(grad_conv)
    later = passed_along(grad_conv[: taps - 1], SP, -1)
    own_grad = grad_conv.astype(jnp.float32)
    tap_list = []
    for offset in range(taps):
        tap_list.append(jnp.sum(own_grad * padded_in[offset : offset + rows_here], 0))
    tail = dense(jnp.stack(tap_list + [gain_part], 0))
    tail = from_everyone(tail, "sp_1").sum(axis=0).astype(jnp.bfloat16)
    near, far = (lax.axis_size("z_near"), lax.axis_size("z_far"))
    part = weight_part.reshape(far, near, -1, weight_part.shape[-1]).transpose(1, 0, 2, 3)
    part = part.reshape(near, -1, weight_part.shape[-1])
    sums = jnp.concatenate([part, jnp.broadcast_to(tail, (near, *tail.shape))], 1)
    sums = exchange(sums, "z_near").astype(jnp.float32).sum(axis=0).astype(jnp.bfloat16)
    tail = sums[part.shape[1] :]
    part = sums[: part.shape[1]].reshape(far, -1, weight_part.shape[-1])
    sums = jnp.concatenate([part, jnp.broadcast_to(tail, (far, *tail.shape))], 1)
    sums = exchange(sums, "z_far").astype(jnp.float32).sum(axis=0)
    grad_out_weight = undense(sums[: part.shape[1]])
    tail = undense(sums[part.shape[1] :])
    grad_taps, grad_gain = (tail[:taps], tail[taps])

    padded_grad = jnp.concatenate([grad_conv, later], 0).astype(jnp.float32)
    grad_mixed = jnp.zeros((rows_here, width_dp), jnp.float32)
    for offset in range(taps):
        back = taps - 1 - offset
        grad_mixed = grad_mixed + conv_taps[offset][None, :] * padded_grad[back : back + rows_here]
    grad_rows = lax.optimization_barrier(grad_mixed.astype(jnp.bfloat16)).astype(jnp.float32)
    grad_val = (grad_rows * sigma_gate).astype(jnp.bfloat16)
    grad_gate = (
        grad_rows * val_input.astype(jnp.float32) * sigma_gate * (1.0 - sigma_gate)
    ).astype(jnp.bfloat16)
    return (grad_val, grad_gate, grad_out_weight, grad_taps, grad_gain)


def solution(mesh):
    split = Mesh(mesh.devices.reshape(4, 4, 4, mesh.shape["dp"]), (*SP, "dp"))
    in_specs = (P(SP, "dp"), P(SP, "dp"), P(SP, None), P(SP, "dp"), P(None, "dp"), P("dp"))
    out_specs = (P(SP, "dp"), P(SP, "dp"), P(SP, "dp"), P(None, "dp"), P("dp"))

    return jax.shard_map(
        per_device, mesh=split, in_specs=in_specs, out_specs=out_specs, check_vma=False
    )
```

profile of v0, /device:TPU:56, one launch (start us, length us, event | category | flops | bytes accessed | tf_op | source)
XLA Modules:
  0.0 129.4 jit_solution(17761565017989266213)
XLA Ops:
  0.7 0.8 fusion.113
  1.5 0.7 slice.456
  2.3 0.8 broadcast_in_dim.20
  3.1 15.2 %all-to-all-start = ((bf16[16,96,128]{2,1,0:T(8,128)(2,1)}), bf16[16,96,128]{2,1,0:T(8,128)(2,1)S(1)}, u32[]{:S(2)}, u32[]{:S(2)}) async-start(bf16[16,96,128]{2,1,0:T(8,128)(2,1)} %broadcast_in_dim.20), calls=%async_computation | async-start | bytes 786432 | tf_op jit(solution)/shard_map/all_to_all | solution.py:22
  18.4 3.0 %collective-permute-start = (bf16[30,192]{0,1:T(8,128)(2,1)S(1)}, bf16[30,192]{0,1:T(8,128)(2,1)S(1)}, u32[]{:S(2)}, u32[]{:S(2)}) collective-permute-start(bf16[30,192]{0,1:T(8,128)(2,1)S(1)} %slice.581), channel_id=1, source_target_pairs={{0,8},{8,16},{16,24},{24,32},{32,40},{40,48},{48,56},{56,64},{64,7... | collective-permute-start | bytes 34568 | tf_op jit(solution)/shard_map/ppermute | solution.py:18
  21.5 0.7 copy.20
  22.4 3.6 %collective-permute-start.2 = (bf16[128,1024]{0,1:T(8,128)(2,1)S(1)}, bf16[128,1024]{0,1:T(8,128)(2,1)S(1)}, u32[]{:S(2)}, u32[]{:S(2)}) collective-permute-start(bf16[128,1024]{0,1:T(8,128)(2,1)S(1)} %get-tuple-element.48), channel_id=1, source_target_pairs={{0,16},{8,24},{16,0},{24,8},{1,17},{9,25},{17,1},{25,9},{2,18},{10... | collective-permute-start | bytes 786440 | tf_op jit(solution)/shard_map/ppermute | solution.py:30
  26.0 1.9 %collective-permute-start.3 = (bf16[128,1024]{0,1:T(8,128)(2,1)S(1)}, bf16[128,1024]{0,1:T(8,128)(2,1)S(1)}, u32[]{:S(2)}, u32[]{:S(2)}) collective-permute-start(bf16[128,1024]{0,1:T(8,128)(2,1)S(1)} %get-tuple-element.46), channel_id=1, source_target_pairs={{0,8},{8,0},{16,24},{24,16},{1,9},{9,1},{17,25},{25,17},{2,10},{10... | collective-permute-start | bytes 786440 | tf_op jit(solution)/shard_map/ppermute | solution.py:30
  27.9 4.3 %collective-permute-start.1 = (bf16[128,1024]{0,1:T(8,128)(2,1)S(1)}, bf16[128,1024]{0,1:T(8,128)(2,1)}, u32[]{:S(2)}, u32[]{:S(2)}) collective-permute-start(bf16[128,1024]{0,1:T(8,128)(2,1)S(1)} %get-tuple-element.49), channel_id=1, source_target_pairs={{0,24},{8,16},{16,8},{24,0},{1,25},{9,17},{17,9},{25,1},{2,26},{10... | collective-permute-start | bytes 786440 | tf_op jit(solution)/shard_map/ppermute | solution.py:30
  32.5 1.9 %collective-permute-done = bf16[30,192]{0,1:T(8,128)(2,1)S(1)} collective-permute-done((bf16[30,192]{0,1:T(8,128)(2,1)S(1)}, bf16[30,192]{0,1:T(8,128)(2,1)S(1)}, u32[]{:S(2)}, u32[]{:S(2)}) %collective-permute-start) | collective-permute-done | bytes 11552 | tf_op jit(solution)/shard_map/ppermute | solution.py:18
  34.5 1.8 %add_convert_fusion = bf16[128,192]{0,1:T(8,128)(2,1)S(1)} fusion(f32[158,192]{0,1:T(8,128)S(1)} %maximum_convert_fusion, f32[192]{0:T(256)S(1)} %bitcast.198, f32[192]{0:T(256)S(1)} %bitcast.200, f32[192]{0:T(256)S(1)} %bitcast.142, f32[192]{0:T(256)S(1)} %bitcast.144, f32[192]{0:T(256)S(1)} %bitcast.146, f32[192]{0:T(256)S(1)} %bitcast.148, ...), kind=kLoop, calls=%fused_computation.195 | loop fusion | flops 1523712 | bytes 3120384 | tf_op jit(solution)/shard_map/convert_element_type | solution.py:81
  36.6 4.9 %all-to-all-done = bf16[16,96,128]{2,1,0:T(8,128)(2,1)S(1)} async-done(((bf16[16,96,128]{2,1,0:T(8,128)(2,1)}), bf16[16,96,128]{2,1,0:T(8,128)(2,1)S(1)}, u32[]{:S(2)}, u32[]{:S(2)}) %all-to-all-start) | async-done | bytes 393248 | tf_op jit(solution)/shard_map/all_to_all | solution.py:22
  41.5 0.1 fusion.110
  41.7 0.6 broadcast_in_dim.21
  42.3 4.3 %all-to-all-start.1 = ((f32[8,2,128]{2,1,0:T(2,128)}), f32[8,2,128]{2,1,0:T(2,128)S(1)}, u32[]{:S(2)}, u32[]{:S(2)}) async-start(f32[8,2,128]{2,1,0:T(2,128)} %broadcast_in_dim.21), calls=%async_computation.1 | async-start | bytes 16384 | tf_op jit(solution)/shard_map/all_to_all | solution.py:22
  46.6 0.1 maximum_maximum_fusion
  46.7 0.3 convolution_convert_fusion.1
  47.0 0.3 convolution_convert_fusion.3
  47.4 0.3 convolution_convert_fusion.2
  47.7 1.3 broadcast_select_fusion.11
  49.0 2.9 %all-to-all-done.1 = f32[8,2,128]{2,1,0:T(2,128)S(1)} async-done(((f32[8,2,128]{2,1,0:T(2,128)}), f32[8,2,128]{2,1,0:T(2,128)S(1)}, u32[]{:S(2)}, u32[]{:S(2)}) %all-to-all-start.1) | async-done | bytes 8224 | tf_op jit(solution)/shard_map/all_to_all | solution.py:22
  51.9 0.1 fusion.35
  52.2 10.3 %all_to_all.35 = bf16[4,128,384]{1,2,0:T(8,128)(2,1)S(1)} all-to-all(bf16[4,128,384]{1,2,0:T(8,128)(2,1)S(1)} %pad_maximum_fusion.1), channel_id=1, replica_groups=mesh['z_far'=4,'z_near'=4,'sp_1'=4,'dp'=8] {'sp_1'}, dimensions={0} | all-to-all | bytes 786432 | tf_op jit(solution)/shard_map/all_to_all | solution.py:22
  62.5 0.2 fusion.42
  62.7 0.6 broadcast_in_dim.22
  63.3 3.3 %all-to-all-start.3 = ((f32[8,2,128]{2,1,0:T(2,128)}), f32[8,2,128]{2,1,0:T(2,128)S(1)}, u32[]{:S(2)}, u32[]{:S(2)}) async-start(f32[8,2,128]{2,1,0:T(2,128)} %broadcast_in_dim.22), calls=%async_computation.3 | async-start | bytes 16384 | tf_op jit(solution)/shard_map/all_to_all | solution.py:22
  66.7 1.5 %convolution_convert_fusion = bf16[1024,192]{0,1:T(8,128)(2,1)S(1)} fusion(bf16[128,1024]{0,1:T(8,128)(2,1)} %collective-permute-done.1, bf16[128,1024]{0,1:T(8,128)(2,1)S(1)} %collective-permute-done.2, bf16[128,1024]{0,1:T(8,128)(2,1)S(1)} %collective-permute-done.3, bf16[128,1024]{0,1:T(8,128)(2,1)S(1)} %get-tuple-element.47, ...), kind=kOutput, calls=%fused_computation | convolution fusion | flops 206503936 | bytes 1638400 | tf_op jit(solution)/shard_map/dot_general | solution.py:101
  68.2 0.2 copy.23
  68.5 3.4 %all-to-all-done.3 = f32[8,2,128]{2,1,0:T(2,128)S(1)} async-done(((f32[8,2,128]{2,1,0:T(2,128)}), f32[8,2,128]{2,1,0:T(2,128)S(1)}, u32[]{:S(2)}, u32[]{:S(2)}) %all-to-all-start.3) | async-done | bytes 8224 | tf_op jit(solution)/shard_map/all_to_all | solution.py:22
  72.0 1.2 fusion.58
  73.2 0.9 fusion.43
  74.2 0.1 stack.181
  74.4 0.6 broadcast_in_dim.23
  75.1 5.3 %all-to-all-start.4 = ((f32[4,48,128]{2,1,0:T(8,128)}), f32[4,48,128]{2,1,0:T(8,128)S(1)}, u32[]{:S(2)}, u32[]{:S(2)}) async-start(f32[4,48,128]{2,1,0:T(8,128)} %broadcast_in_dim.23), calls=%async_computation.4 | async-start | bytes 196608 | tf_op jit(solution)/shard_map/all_to_all | solution.py:22
  80.4 0.1 maximum_maximum_fusion.1
  80.6 3.6 %all-to-all-done.4 = f32[4,48,128]{2,1,0:T(8,128)S(1)} async-done(((f32[4,48,128]{2,1,0:T(8,128)}), f32[4,48,128]{2,1,0:T(8,128)S(1)}, u32[]{:S(2)}, u32[]{:S(2)}) %all-to-all-start.4) | async-done | bytes 98336 | tf_op jit(solution)/shard_map/all_to_all | solution.py:22
  84.2 0.8 pad_maximum_fusion
  85.0 5.8 %all-to-all-start.5 = ((bf16[4,432,128]{2,1,0:T(8,128)(2,1)}), bf16[4,432,128]{2,1,0:T(8,128)(2,1)S(1)}, u32[]{:S(2)}, u32[]{:S(2)}) async-start(bf16[4,432,128]{2,1,0:T(8,128)(2,1)} %pad_maximum_fusion), calls=%async_computation.5 | async-start | bytes 884736 | tf_op jit(solution)/shard_map/all_to_all | solution.py:22
  91.0 2.2 %collective-permute-start.4 = (bf16[30,192]{0,1:T(8,128)(2,1)S(1)}, bf16[30,192]{0,1:T(8,128)(2,1)S(1)}, u32[]{:S(2)}, u32[]{:S(2)}) collective-permute-start(bf16[30,192]{0,1:T(8,128)(2,1)S(1)} %bitcast.137), channel_id=1, source_target_pairs={{8,0},{16,8},{24,16},{32,24},{40,32},{48,40},{56,48},{64,56},{72,6... | collective-permute-start | bytes 34568 | tf_op jit(solution)/shard_map/ppermute | solution.py:18
  93.2 10.5 %collective-permute-done.4 = bf16[30,192]{0,1:T(8,128)(2,1)S(1)} collective-permute-done((bf16[30,192]{0,1:T(8,128)(2,1)S(1)}, bf16[30,192]{0,1:T(8,128)(2,1)S(1)}, u32[]{:S(2)}, u32[]{:S(2)}) %collective-permute-start.4) | collective-permute-done | bytes 11552 | tf_op jit(solution)/shard_map/ppermute | solution.py:18
  103.9 0.7 pad_maximum_fusion.2
  104.5 8.5 %all-to-all-start.6 = ((bf16[4,144,128]{2,1,0:T(8,128)(2,1)}), bf16[4,144,128]{2,1,0:T(8,128)(2,1)S(1)}, u32[]{:S(2)}, u32[]{:S(2)}) async-start(bf16[4,144,128]{2,1,0:T(8,128)(2,1)} %pad_maximum_fusion.2), calls=%async_computation.6 | async-start | bytes 294912 | tf_op jit(solution)/shard_map/all_to_all | solution.py:22
  113.2 1.8 %fusion.75 = bf16[128,192]{0,1:T(8,128)(2,1)S(1)} fusion(f32[158,192]{0,1:T(8,128)S(1)} %maximum_convert_fusion.1, f32[192]{0:T(256)S(1)} %bitcast.199, f32[192]{0:T(256)S(1)} %bitcast.201, f32[192]{0:T(256)S(1)} %bitcast.143, f32[192]{0:T(256)S(1)} %bitcast.145, f32[192]{0:T(256)S(1)} %bitcast.147, f32[192]{0:T(256)S(1)} %bitcast.149, ...), kind=kLoop, calls=%fused_computation.133 | loop fusion | flops 1523712 | bytes 3120384 | tf_op jit(solution)/shard_map/convert_element_type | solution.py:143
  115.0 0.7 fusion.18
  115.7 11.7 %all-to-all-done.6 = bf16[4,144,128]{2,1,0:T(8,128)(2,1)S(1)} async-done(((bf16[4,144,128]{2,1,0:T(8,128)(2,1)}), bf16[4,144,128]{2,1,0:T(8,128)(2,1)S(1)}, u32[]{:S(2)}, u32[]{:S(2)}) %all-to-all-start.6) | async-done | bytes 147488 | tf_op jit(solution)/shard_map/all_to_all | solution.py:22
  127.6 0.6 maximum_maximum_fusion.3
  128.2 0.6 pad_maximum_fusion.7
  128.8 0.6 maximum_maximum_fusion.2
  (149 shorter events, 1.7 us)
Async XLA Ops:
  0.6 17.6 %copy-start.1 = (bf16[128,192]{0,1:T(8,128)(2,1)S(1)}, bf16[128,192]{0,1:T(8,128)(2,1)}, u32[]{:S(2)}) copy-start(bf16[128,192]{0,1:T(8,128)(2,1)} %param.6) | copy-start | bytes 147460
  0.6 17.6 %copy-start.2 = (bf16[128,192]{0,1:T(8,128)(2,1)S(1)}, bf16[128,192]{0,1:T(8,128)(2,1)}, u32[]{:S(2)}) copy-start(bf16[128,192]{0,1:T(8,128)(2,1)} %param.7) | copy-start | bytes 147460
  0.7 20.8 %copy-start = (bf16[128,4096]{1,0:T(8,128)(2,1)S(1)}, bf16[128,4096]{1,0:T(8,128)(2,1)}, u32[]{:S(2)}) copy-start(bf16[128,4096]{1,0:T(8,128)(2,1)} %param.8) | copy-start | bytes 3145732
  3.1 38.5 %all-to-all-start = ((bf16[16,96,128]{2,1,0:T(8,128)(2,1)}), bf16[16,96,128]{2,1,0:T(8,128)(2,1)S(1)}, u32[]{:S(2)}, u32[]{:S(2)}) async-start(bf16[16,96,128]{2,1,0:T(8,128)(2,1)} %broadcast_in_dim.20), calls=%async_computation | async-start | bytes 786432 | tf_op jit(solution)/shard_map/all_to_all | solution.py:22
  18.4 16.0 %collective-permute-start = (bf16[30,192]{0,1:T(8,128)(2,1)S(1)}, bf16[30,192]{0,1:T(8,128)(2,1)S(1)}, u32[]{:S(2)}, u32[]{:S(2)}) collective-permute-start(bf16[30,192]{0,1:T(8,128)(2,1)S(1)} %slice.581), channel_id=1, source_target_pairs={{0,8},{8,16},{16,24},{24,32},{32,40},{40,48},{48,56},{56,64},{64,7... | collective-permute-start | bytes 34568 | tf_op jit(solution)/shard_map/ppermute | solution.py:18
  22.3 9.9 %copy-start.3 = (f32[31,192]{1,0:T(8,128)S(1)}, f32[31,192]{1,0:T(8,128)}, u32[]{:S(2)}) copy-start(f32[31,192]{1,0:T(8,128)} %param.10) | copy-start | bytes 71428
  22.4 24.7 %collective-permute-start.2 = (bf16[128,1024]{0,1:T(8,128)(2,1)S(1)}, bf16[128,1024]{0,1:T(8,128)(2,1)S(1)}, u32[]{:S(2)}, u32[]{:S(2)}) collective-permute-start(bf16[128,1024]{0,1:T(8,128)(2,1)S(1)} %get-tuple-element.48), channel_id=1, source_target_pairs={{0,16},{8,24},{16,0},{24,8},{1,17},{9,25},{17,1},{25,9},{2,18},{10... | collective-permute-start | bytes 786440 | tf_op jit(solution)/shard_map/ppermute | solution.py:30
  26.0 21.4 %collective-permute-start.3 = (bf16[128,1024]{0,1:T(8,128)(2,1)S(1)}, bf16[128,1024]{0,1:T(8,128)(2,1)S(1)}, u32[]{:S(2)}, u32[]{:S(2)}) collective-permute-start(bf16[128,1024]{0,1:T(8,128)(2,1)S(1)} %get-tuple-element.46), channel_id=1, source_target_pairs={{0,8},{8,0},{16,24},{24,16},{1,9},{9,1},{17,25},{25,17},{2,10},{10... | collective-permute-start | bytes 786440 | tf_op jit(solution)/shard_map/ppermute | solution.py:30
  27.9 19.8 %collective-permute-start.1 = (bf16[128,1024]{0,1:T(8,128)(2,1)S(1)}, bf16[128,1024]{0,1:T(8,128)(2,1)}, u32[]{:S(2)}, u32[]{:S(2)}) collective-permute-start(bf16[128,1024]{0,1:T(8,128)(2,1)S(1)} %get-tuple-element.49), channel_id=1, source_target_pairs={{0,24},{8,16},{16,8},{24,0},{1,25},{9,17},{17,9},{25,1},{2,26},{10... | collective-permute-start | bytes 786440 | tf_op jit(solution)/shard_map/ppermute | solution.py:30
  32.2 4.1 %copy-start.4 = (f32[1,192]{1,0:T(1,128)}, f32[1,192]{1,0:T(1,128)S(1)}, u32[]{:S(2)}) copy-start(f32[1,192]{1,0:T(1,128)S(1)} %get-tuple-element.82) | copy-start | bytes 2308
  32.3 4.1 %copy-start.6 = (f32[1,192]{1,0:T(1,128)}, f32[1,192]{1,0:T(1,128)S(1)}, u32[]{:S(2)}) copy-start(f32[1,192]{1,0:T(1,128)S(1)} %get-tuple-element.83) | copy-start | bytes 2308
  32.3 4.1 %copy-start.8 = (f32[1,192]{1,0:T(1,128)}, f32[1,192]{1,0:T(1,128)S(1)}, u32[]{:S(2)}) copy-start(f32[1,192]{1,0:T(1,128)S(1)} %get-tuple-element.84) | copy-start | bytes 2308
  32.3 4.1 %copy-start.10 = (f32[1,192]{1,0:T(1,128)}, f32[1,192]{1,0:T(1,128)S(1)}, u32[]{:S(2)}) copy-start(f32[1,192]{1,0:T(1,128)S(1)} %get-tuple-element.85) | copy-start | bytes 2308
  32.3 4.1 %copy-start.12 = (f32[1,192]{1,0:T(1,128)}, f32[1,192]{1,0:T(1,128)S(1)}, u32[]{:S(2)}) copy-start(f32[1,192]{1,0:T(1,128)S(1)} %get-tuple-element.86) | copy-start | bytes 2308
  32.3 4.1 %copy-start.14 = (f32[1,192]{1,0:T(1,128)}, f32[1,192]{1,0:T(1,128)S(1)}, u32[]{:S(2)}) copy-start(f32[1,192]{1,0:T(1,128)S(1)} %get-tuple-element.87) | copy-start | bytes 2308
  32.3 4.1 %copy-start.16 = (f32[1,192]{1,0:T(1,128)}, f32[1,192]{1,0:T(1,128)S(1)}, u32[]{:S(2)}) copy-start(f32[1,192]{1,0:T(1,128)S(1)} %get-tuple-element.88) | copy-start | bytes 2308
  32.3 4.1 %copy-start.18 = (f32[1,192]{1,0:T(1,128)}, f32[1,192]{1,0:T(1,128)S(1)}, u32[]{:S(2)}) copy-start(f32[1,192]{1,0:T(1,128)S(1)} %get-tuple-element.89) | copy-start | bytes 2308
  32.3 4.1 %copy-start.20 = (f32[1,192]{1,0:T(1,128)}, f32[1,192]{1,0:T(1,128)S(1)}, u32[]{:S(2)}) copy-start(f32[1,192]{1,0:T(1,128)S(1)} %get-tuple-element.90) | copy-start | bytes 2308
  42.3 9.6 %all-to-all-start.1 = ((f32[8,2,128]{2,1,0:T(2,128)}), f32[8,2,128]{2,1,0:T(2,128)S(1)}, u32[]{:S(2)}, u32[]{:S(2)}) async-start(f32[8,2,128]{2,1,0:T(2,128)} %broadcast_in_dim.21), calls=%async_computation.1 | async-start | bytes 16384 | tf_op jit(solution)/shard_map/all_to_all | solution.py:22
  47.4 4.6 %copy-start.50 = (f32[192]{0:T(256)S(1)}, f32[192]{0:T(256)}, u32[]{:S(2)}) copy-start(f32[192]{0:T(256)} %param.11) | copy-start | bytes 2308
  63.3 8.6 %all-to-all-start.3 = ((f32[8,2,128]{2,1,0:T(2,128)}), f32[8,2,128]{2,1,0:T(2,128)S(1)}, u32[]{:S(2)}, u32[]{:S(2)}) async-start(f32[8,2,128]{2,1,0:T(2,128)} %broadcast_in_dim.22), calls=%async_computation.3 | async-start | bytes 16384 | tf_op jit(solution)/shard_map/all_to_all | solution.py:22
  75.1 9.1 %all-to-all-start.4 = ((f32[4,48,128]{2,1,0:T(8,128)}), f32[4,48,128]{2,1,0:T(8,128)S(1)}, u32[]{:S(2)}, u32[]{:S(2)}) async-start(f32[4,48,128]{2,1,0:T(8,128)} %broadcast_in_dim.23), calls=%async_computation.4 | async-start | bytes 196608 | tf_op jit(solution)/shard_map/all_to_all | solution.py:22
  85.0 18.8 %all-to-all-start.5 = ((bf16[4,432,128]{2,1,0:T(8,128)(2,1)}), bf16[4,432,128]{2,1,0:T(8,128)(2,1)S(1)}, u32[]{:S(2)}, u32[]{:S(2)}) async-start(bf16[4,432,128]{2,1,0:T(8,128)(2,1)} %pad_maximum_fusion), calls=%async_computation.5 | async-start | bytes 884736 | tf_op jit(solution)/shard_map/all_to_all | solution.py:22
  90.8 22.2 %copy-start.5 = (f32[1,192]{1,0:T(1,128)S(1)}, f32[1,192]{1,0:T(1,128)}, u32[]{:S(2)}) copy-start(f32[1,192]{1,0:T(1,128)} %copy-done.4) | copy-start | bytes 2308
  90.8 22.2 %copy-start.7 = (f32[1,192]{1,0:T(1,128)S(1)}, f32[1,192]{1,0:T(1,128)}, u32[]{:S(2)}) copy-start(f32[1,192]{1,0:T(1,128)} %copy-done.6) | copy-start | bytes 2308
  90.8 22.2 %copy-start.9 = (f32[1,192]{1,0:T(1,128)S(1)}, f32[1,192]{1,0:T(1,128)}, u32[]{:S(2)}) copy-start(f32[1,192]{1,0:T(1,128)} %copy-done.8) | copy-start | bytes 2308
  90.8 22.2 %copy-start.11 = (f32[1,192]{1,0:T(1,128)S(1)}, f32[1,192]{1,0:T(1,128)}, u32[]{:S(2)}) copy-start(f32[1,192]{1,0:T(1,128)} %copy-done.10) | copy-start | bytes 2308
  90.8 22.2 %copy-start.13 = (f32[1,192]{1,0:T(1,128)S(1)}, f32[1,192]{1,0:T(1,128)}, u32[]{:S(2)}) copy-start(f32[1,192]{1,0:T(1,128)} %copy-done.12) | copy-start | bytes 2308
  90.8 22.2 %copy-start.15 = (f32[1,192]{1,0:T(1,128)S(1)}, f32[1,192]{1,0:T(1,128)}, u32[]{:S(2)}) copy-start(f32[1,192]{1,0:T(1,128)} %copy-done.14) | copy-start | bytes 2308
  90.8 22.2 %copy-start.17 = (f32[1,192]{1,0:T(1,128)S(1)}, f32[1,192]{1,0:T(1,128)}, u32[]{:S(2)}) copy-start(f32[1,192]{1,0:T(1,128)} %copy-done.16) | copy-start | bytes 2308
  90.8 22.2 %copy-start.19 = (f32[1,192]{1,0:T(1,128)S(1)}, f32[1,192]{1,0:T(1,128)}, u32[]{:S(2)}) copy-start(f32[1,192]{1,0:T(1,128)} %copy-done.18) | copy-start | bytes 2308
  90.8 22.2 %copy-start.21 = (f32[1,192]{1,0:T(1,128)S(1)}, f32[1,192]{1,0:T(1,128)}, u32[]{:S(2)}) copy-start(f32[1,192]{1,0:T(1,128)} %copy-done.20) | copy-start | bytes 2308
  90.8 22.2 %copy-start.23 = (f32[1,192]{1,0:T(1,128)S(1)}, f32[1,192]{1,0:T(1,128)}, u32[]{:S(2)}) copy-start(f32[1,192]{1,0:T(1,128)} %copy-done.22) | copy-start | bytes 2308
  90.9 22.2 %copy-start.25 = (f32[1,192]{1,0:T(1,128)S(1)}, f32[1,192]{1,0:T(1,128)}, u32[]{:S(2)}) copy-start(f32[1,192]{1,0:T(1,128)} %copy-done.24) | copy-start | bytes 2308
  90.9 22.2 %copy-start.27 = (f32[1,192]{1,0:T(1,128)S(1)}, f32[1,192]{1,0:T(1,128)}, u32[]{:S(2)}) copy-start(f32[1,192]{1,0:T(1,128)} %copy-done.26) | copy-start | bytes 2308
  90.9 22.2 %copy-start.29 = (f32[1,192]{1,0:T(1,128)S(1)}, f32[1,192]{1,0:T(1,128)}, u32[]{:S(2)}) copy-start(f32[1,192]{1,0:T(1,128)} %copy-done.28) | copy-start | bytes 2308
  90.9 22.2 %copy-start.31 = (f32[1,192]{1,0:T(1,128)S(1)}, f32[1,192]{1,0:T(1,128)}, u32[]{:S(2)}) copy-start(f32[1,192]{1,0:T(1,128)} %copy-done.30) | copy-start | bytes 2308
  90.9 22.2 %copy-start.33 = (f32[1,192]{1,0:T(1,128)S(1)}, f32[1,192]{1,0:T(1,128)}, u32[]{:S(2)}) copy-start(f32[1,192]{1,0:T(1,128)} %copy-done.32) | copy-start | bytes 2308
  90.9 22.2 %copy-start.35 = (f32[1,192]{1,0:T(1,128)S(1)}, f32[1,192]{1,0:T(1,128)}, u32[]{:S(2)}) copy-start(f32[1,192]{1,0:T(1,128)} %copy-done.34) | copy-start | bytes 2308
  90.9 22.2 %copy-start.37 = (f32[1,192]{1,0:T(1,128)S(1)}, f32[1,192]{1,0:T(1,128)}, u32[]{:S(2)}) copy-start(f32[1,192]{1,0:T(1,128)} %copy-done.36) | copy-start | bytes 2308
  90.9 22.2 %copy-start.39 = (f32[1,192]{1,0:T(1,128)S(1)}, f32[1,192]{1,0:T(1,128)}, u32[]{:S(2)}) copy-start(f32[1,192]{1,0:T(1,128)} %copy-done.38) | copy-start | bytes 2308
  90.9 22.2 %copy-start.41 = (f32[1,192]{1,0:T(1,128)S(1)}, f32[1,192]{1,0:T(1,128)}, u32[]{:S(2)}) copy-start(f32[1,192]{1,0:T(1,128)} %copy-done.40) | copy-start | bytes 2308
  90.9 22.2 %copy-start.43 = (f32[1,192]{1,0:T(1,128)S(1)}, f32[1,192]{1,0:T(1,128)}, u32[]{:S(2)}) copy-start(f32[1,192]{1,0:T(1,128)} %copy-done.42) | copy-start | bytes 2308
  91.0 22.2 %copy-start.45 = (f32[1,192]{1,0:T(1,128)S(1)}, f32[1,192]{1,0:T(1,128)}, u32[]{:S(2)}) copy-start(f32[1,192]{1,0:T(1,128)} %copy-done.44) | copy-start | bytes 2308
  91.0 22.2 %copy-start.47 = (f32[1,192]{1,0:T(1,128)S(1)}, f32[1,192]{1,0:T(1,128)}, u32[]{:S(2)}) copy-start(f32[1,192]{1,0:T(1,128)} %copy-done.46) | copy-start | bytes 2308
  91.0 22.2 %copy-start.49 = (f32[1,192]{1,0:T(1,128)S(1)}, f32[1,192]{1,0:T(1,128)}, u32[]{:S(2)}) copy-start(f32[1,192]{1,0:T(1,128)} %copy-done.48) | copy-start | bytes 2308
  91.0 12.7 %collective-permute-start.4 = (bf16[30,192]{0,1:T(8,128)(2,1)S(1)}, bf16[30,192]{0,1:T(8,128)(2,1)S(1)}, u32[]{:S(2)}, u32[]{:S(2)}) collective-permute-start(bf16[30,192]{0,1:T(8,128)(2,1)S(1)} %bitcast.137), channel_id=1, source_target_pairs={{8,0},{16,8},{24,16},{32,24},{40,32},{48,40},{56,48},{64,56},{72,6... | collective-permute-start | bytes 34568 | tf_op jit(solution)/shard_map/ppermute | solution.py:18
  104.5 22.9 %all-to-all-start.6 = ((bf16[4,144,128]{2,1,0:T(8,128)(2,1)}), bf16[4,144,128]{2,1,0:T(8,128)(2,1)S(1)}, u32[]{:S(2)}, u32[]{:S(2)}) async-start(bf16[4,144,128]{2,1,0:T(8,128)(2,1)} %pad_maximum_fusion.2), calls=%async_computation.6 | async-start | bytes 294912 | tf_op jit(solution)/shard_map/all_to_all | solution.py:22
  (14 other events, 57.0 us)
where the time goes:
time: 130 us; the launch traced here: 129 us
  starting transfers between devices  57.5 us (44%)
  waiting for transfers between devices  38.9 us (30%)
  other arithmetic  11 us (8%)
  blocking collectives  10.3 us (8%)
  local copies, waits for them, and re-layouts  6.19 us (5%)
  matrix products  3.72 us (3%)
  between operations  1.81 us (1%)
    all_to_all x6, starting transfers between devices, exchange(): return lax.all_to_all(blocks, axis, split_axis=0, concat_axis=0, tiled=True)  42.5 us
    all_to_all x6, waiting for transfers between devices, exchange(): return lax.all_to_all(blocks, axis, split_axis=0, concat_axis=0, tiled=True)  26.5 us
    ppermute x2, waiting for transfers between devices, passed_along(): lax.ppermute(value, axis, [(source, source + steps) for source in range(f...  12.4 us
    all_to_all x1, blocking collectives, exchange(): return lax.all_to_all(blocks, axis, split_axis=0, concat_axis=0, tiled=True)  10.3 us
    ppermute x3, starting transfers between devices, swapped(): lax.ppermute(value, axis, [(i, i ^ k) for i in range(lax.axis_size(axis))])  9.82 us
    ppermute x2, starting transfers between devices, passed_along(): lax.ppermute(value, axis, [(source, source + steps) for source in range(f...  5.24 us
    broadcast_in_dim x4, local copies, waits for them, and re-layouts, from_everyone(): jnp.broadcast_to(array, (lax.axis_size(axis), *array.shape))  2.63 us
  transfers between devices with their start and end apart: 11, of which 7 were waited for; matrix products, arithmetic and copies ran while one was open for 8% of the time, Pallas kernels for 0%

commit v1 on v0

--- a/solution.py
+++ b/solution.py
@@ -1,6 +1,7 @@
 import jax
 import jax.numpy as jnp
 from jax import lax
+from jax.experimental.layout import Layout, with_layout_constraint
 from jax.sharding import Mesh
 from jax.sharding import PartitionSpec as P
 
@@ -26,6 +27,18 @@
     return exchange(jnp.broadcast_to(array, (lax.axis_size(axis), *array.shape)), axis)
 
 
+def packed(rows):
+    turned = rows.T
+    quarter = turned.shape[0] // 4
+    return jnp.concatenate([turned[quarter * j : quarter * (j + 1)] for j in range(4)], 1)
+
+
+def unpacked(block):
+    tokens = block.shape[1] // 4
+    parts = [block[:, tokens * j : tokens * (j + 1)] for j in range(4)]
+    return jnp.concatenate(parts, 0).T
+
+
 def swapped(value, axis, k):
     return lax.ppermute(value, axis, [(i, i ^ k) for i in range(lax.axis_size(axis))])
 
@@ -37,6 +50,10 @@
         blocks = [jnp.where(swap, blocks[j ^ k], blocks[j]) for j in range(len(blocks))]
         k *= 2
     return blocks
+
+
+def tokens_major(array):
+    return with_layout_constraint(array, Layout(major_to_minor=(0, 1)))
 
 
 def dense(blocks):
@@ -71,7 +88,8 @@
 
     sigma_gate = jax.nn.sigmoid(gate_input.astype(jnp.float32))
     mixed_in = (val_input.astype(jnp.float32) * sigma_gate).astype(jnp.bfloat16)
-    earlier = passed_along(mixed_in[rows_here - (taps - 1) :], SP, 1)
+    earlier = passed_along(packed(mixed_in[rows_here - (taps + 1) :]), SP, 1)
+    earlier = unpacked(earlier)[2:]
     padded_in = jnp.concatenate([earlier, lax.optimization_barrier(mixed_in)], 0).astype(
         jnp.float32
     )
@@ -105,6 +123,12 @@
         preferred_element_type=jnp.float32,
     )
     weight_part = dense(weight_part.astype(jnp.bfloat16).reshape(z_size, d_rows, width_dp))
+    near, far = (lax.axis_size("z_near"), lax.axis_size("z_far"))
+    near_here = lax.axis_index("z_near")
+    part = weight_part.reshape(far, near, -1, weight_part.shape[-1])
+    part = [lax.dynamic_index_in_dim(part, near_here ^ k, 1, False) for k in range(near)]
+    arrived = [swapped(part[near - 1], "z_near", near - 1)]
+    arrived += [swapped(part[k], "z_near", k) for k in range(1, near - 1)]
 
     grad_act = grad_mix * sigma_act * (1.0 + act * (1.0 - sigma_act))
     gain_part = jnp.sum(grad_act * normed, 0)
@@ -116,21 +140,19 @@
     grad_conv = (inv_scale * (grad_norm - first_sum - normed * second_sum)).astype(jnp.bfloat16)
     grad_conv = lax.optimization_barrier(grad_conv)
     later = passed_along(grad_conv[: taps - 1], SP, -1)
-    own_grad = grad_conv.astype(jnp.float32)
+    own_grad = tokens_major(grad_conv).astype(jnp.float32)
+    tap_rows = tokens_major(padded_in.astype(jnp.bfloat16)).astype(jnp.float32)
     tap_list = []
     for offset in range(taps):
-        tap_list.append(jnp.sum(own_grad * padded_in[offset : offset + rows_here], 0))
-    tail = dense(jnp.stack(tap_list + [gain_part], 0))
-    tail = from_everyone(tail, "sp_1").sum(axis=0).astype(jnp.bfloat16)
-    near, far = (lax.axis_size("z_near"), lax.axis_size("z_far"))
-    part = weight_part.reshape(far, near, -1, weight_part.shape[-1]).transpose(1, 0, 2, 3)
-    part = part.reshape(near, -1, weight_part.shape[-1])
-    sums = jnp.concatenate([part, jnp.broadcast_to(tail, (near, *tail.shape))], 1)
-    sums = exchange(sums, "z_near").astype(jnp.float32).sum(axis=0).astype(jnp.bfloat16)
-    tail = sums[part.shape[1] :]
-    part = sums[: part.shape[1]].reshape(far, -1, weight_part.shape[-1])
+        tap_list.append(jnp.sum(own_grad * tap_rows[offset : offset + rows_here], 0))
+    tail = dense(jnp.stack(tap_list + [gain_part], 0)).astype(jnp.bfloat16)
+    tail = from_everyone(tail, ("z_near", "sp_1"))
+    tail = tail.astype(jnp.float32).sum(axis=0).astype(jnp.bfloat16)
+    part = sum([p.astype(jnp.float32) for p in arrived], part[0].astype(jnp.float32))
+    part = part.astype(jnp.bfloat16)
     sums = jnp.concatenate([part, jnp.broadcast_to(tail, (far, *tail.shape))], 1)
-    sums = exchange(sums, "z_far").astype(jnp.float32).sum(axis=0)
+    sums = exchange(sums, "z_far")
+    sums = sums.astype(jnp.float32).sum(axis=0)
     grad_out_weight = undense(sums[: part.shape[1]])
     tail = undense(sums[part.shape[1] :])
     grad_taps, grad_gain = (tail[:taps], tail[taps])

time: 130 us -> 131 us (level)
  the two profiles are of different devices: /device:TPU:56 before, /device:TPU:64 now
where the time goes in v1:
time: 131 us; the launch traced here: 130 us
  starting transfers between devices  66.6 us (51%)
  waiting for transfers between devices  44 us (34%)
  local copies, waits for them, and re-layouts  9.7 us (7%)
  other arithmetic  6.37 us (5%)
  between operations  2.18 us (2%)
  matrix products  1.6 us (1%)
    all_to_all x6, waiting for transfers between devices, exchange(): return lax.all_to_all(blocks, axis, split_axis=0, concat_axis=0, tiled=True)  39.9 us
    all_to_all x6, starting transfers between devices, exchange(): return lax.all_to_all(blocks, axis, split_axis=0, concat_axis=0, tiled=True)  39.4 us
    ppermute x6, starting transfers between devices, swapped(): lax.ppermute(value, axis, [(i, i ^ k) for i in range(lax.axis_size(axis))])  19.2 us
    ppermute x2, starting transfers between devices, passed_along(): lax.ppermute(value, axis, [(source, source + steps) for source in range(f...  8.07 us
    unnamed x119, local copies, waits for them, and re-layouts  4.25 us
    ppermute x6, waiting for transfers between devices, swapped(): lax.ppermute(value, axis, [(i, i ^ k) for i in range(lax.axis_size(axis))])  4.14 us
    broadcast_in_dim x4, local copies, waits for them, and re-layouts, from_everyone(): jnp.broadcast_to(array, (lax.axis_size(axis), *array.shape))  2.7 us
  transfers between devices with their start and end apart: 14, of which 6 were waited for; matrix products, arithmetic and copies ran while one was open for 7% of the time, Pallas kernels for 0%

profile of v1, /device:TPU:64, one launch (start us, length us, event | category | flops | bytes accessed | tf_op | source)
XLA Modules:
  0.0 130.5 jit_solution(18169410756582845238)
XLA Ops:
  0.6 1.0 copy.69
  1.6 0.9 copy.70
  2.7 3.5 %collective-permute-start = (bf16[48,128]{0,1:T(8,128)(2,1)S(1)}, bf16[48,128]{0,1:T(8,128)(2,1)S(1)}, u32[]{:S(2)}, u32[]{:S(2)}) collective-permute-start(bf16[48,128]{0,1:T(8,128)(2,1)S(1)} %pad_maximum_fusion.6), channel_id=1, source_target_pairs={{0,8},{8,16},{16,24},{24,32},{32,40},{40,48},{48,56},{56,64},{64,7... | collective-permute-start | bytes 36872 | tf_op jit(solution)/shard_map/ppermute | solution.py:19
  6.2 0.7 fusion.116
  6.9 0.7 slice.542
  7.7 0.8 broadcast_in_dim.17
  8.5 14.8 %all-to-all-start = ((bf16[16,96,128]{2,1,0:T(8,128)(2,1)}), bf16[16,96,128]{2,1,0:T(8,128)(2,1)S(1)}, u32[]{:S(2)}, u32[]{:S(2)}) async-start(bf16[16,96,128]{2,1,0:T(8,128)(2,1)} %broadcast_in_dim.17), calls=%async_computation | async-start | bytes 786432 | tf_op jit(solution)/shard_map/all_to_all | solution.py:23
  23.3 0.7 copy.72
  24.1 4.8 %collective-permute-start.2 = (bf16[128,1024]{0,1:T(8,128)(2,1)S(1)}, bf16[128,1024]{0,1:T(8,128)(2,1)S(1)}, u32[]{:S(2)}, u32[]{:S(2)}) collective-permute-start(bf16[128,1024]{0,1:T(8,128)(2,1)S(1)} %get-tuple-element.73), channel_id=1, source_target_pairs={{0,16},{8,24},{16,0},{24,8},{1,17},{9,25},{17,1},{25,9},{2,18},{10... | collective-permute-start | bytes 786440 | tf_op jit(solution)/shard_map/ppermute | solution.py:43
  29.0 2.0 %collective-permute-start.3 = (bf16[128,1024]{0,1:T(8,128)(2,1)S(1)}, bf16[128,1024]{0,1:T(8,128)(2,1)S(1)}, u32[]{:S(2)}, u32[]{:S(2)}) collective-permute-start(bf16[128,1024]{0,1:T(8,128)(2,1)S(1)} %get-tuple-element.71), channel_id=1, source_target_pairs={{0,8},{8,0},{16,24},{24,16},{1,9},{9,1},{17,25},{25,17},{2,10},{10... | collective-permute-start | bytes 786440 | tf_op jit(solution)/shard_map/ppermute | solution.py:43
  30.9 3.2 %collective-permute-start.1 = (bf16[128,1024]{0,1:T(8,128)(2,1)S(1)}, bf16[128,1024]{0,1:T(8,128)(2,1)S(1)}, u32[]{:S(2)}, u32[]{:S(2)}) collective-permute-start(bf16[128,1024]{0,1:T(8,128)(2,1)S(1)} %get-tuple-element.74), channel_id=1, source_target_pairs={{0,24},{8,16},{16,8},{24,0},{1,25},{9,17},{17,9},{25,1},{2,26},{10... | collective-permute-start | bytes 786440 | tf_op jit(solution)/shard_map/ppermute | solution.py:43
  34.6 0.4 add_convert_fusion
  35.4 10.6 %all-to-all-done = bf16[16,96,128]{2,1,0:T(8,128)(2,1)S(1)} async-done(((bf16[16,96,128]{2,1,0:T(8,128)(2,1)}), bf16[16,96,128]{2,1,0:T(8,128)(2,1)S(1)}, u32[]{:S(2)}, u32[]{:S(2)}) %all-to-all-start) | async-done | bytes 393248 | tf_op jit(solution)/shard_map/all_to_all | solution.py:23
  46.2 0.6 broadcast_in_dim.18
  46.8 4.3 %all-to-all-start.1 = ((f32[8,2,128]{2,1,0:T(2,128)}), f32[8,2,128]{2,1,0:T(2,128)S(1)}, u32[]{:S(2)}, u32[]{:S(2)}) async-start(f32[8,2,128]{2,1,0:T(2,128)} %broadcast_in_dim.18), calls=%async_computation.1 | async-start | bytes 16384 | tf_op jit(solution)/shard_map/all_to_all | solution.py:23
  51.2 0.3 convolution_convert_fusion.1
  51.5 0.3 convolution_convert_fusion.3
  51.8 0.3 convolution_convert_fusion.2
  52.1 0.3 broadcast_select_fusion.11
  52.3 4.0 %all-to-all-done.1 = f32[8,2,128]{2,1,0:T(2,128)S(1)} async-done(((f32[8,2,128]{2,1,0:T(2,128)}), f32[8,2,128]{2,1,0:T(2,128)S(1)}, u32[]{:S(2)}, u32[]{:S(2)}) %all-to-all-start.1) | async-done | bytes 8224 | tf_op jit(solution)/shard_map/all_to_all | solution.py:23
  56.7 0.8 pad_maximum_fusion
  57.5 4.2 %all-to-all-start.2 = ((bf16[4,128,384]{2,1,0:T(8,128)(2,1)}), bf16[4,128,384]{2,1,0:T(8,128)(2,1)S(1)}, u32[]{:S(2)}, u32[]{:S(2)}) async-start(bf16[4,128,384]{2,1,0:T(8,128)(2,1)} %pad_maximum_fusion), calls=%async_computation.2 | async-start | bytes 786432 | tf_op jit(solution)/shard_map/all_to_all | solution.py:23
  61.7 8.0 %all-to-all-done.2 = bf16[4,128,384]{2,1,0:T(8,128)(2,1)S(1)} async-done(((bf16[4,128,384]{2,1,0:T(8,128)(2,1)}), bf16[4,128,384]{2,1,0:T(8,128)(2,1)S(1)}, u32[]{:S(2)}, u32[]{:S(2)}) %all-to-all-start.2) | async-done | bytes 393248 | tf_op jit(solution)/shard_map/all_to_all | solution.py:23
  69.8 0.2 fusion.41
  70.0 0.6 broadcast_in_dim.19
  70.6 3.3 %all-to-all-start.3 = ((f32[8,2,128]{2,1,0:T(2,128)}), f32[8,2,128]{2,1,0:T(2,128)S(1)}, u32[]{:S(2)}, u32[]{:S(2)}) async-start(f32[8,2,128]{2,1,0:T(2,128)} %broadcast_in_dim.19), calls=%async_computation.3 | async-start | bytes 16384 | tf_op jit(solution)/shard_map/all_to_all | solution.py:23
  74.0 0.1 select_bitcast_fusion.3
  74.1 0.5 convolution_convert_fusion
  74.6 0.2 copy.79
  74.9 4.3 %all-to-all-done.3 = f32[8,2,128]{2,1,0:T(2,128)S(1)} async-done(((f32[8,2,128]{2,1,0:T(2,128)}), f32[8,2,128]{2,1,0:T(2,128)S(1)}, u32[]{:S(2)}, u32[]{:S(2)}) %all-to-all-start.3) | async-done | bytes 8224 | tf_op jit(solution)/shard_map/all_to_all | solution.py:23
  79.4 0.3 fusion.57
  79.7 0.2 fusion.42
  80.6 0.7 broadcast_in_dim.20
  81.3 5.2 %all-to-all-start.4 = ((bf16[16,48,128]{2,1,0:T(8,128)(2,1)}), bf16[16,48,128]{2,1,0:T(8,128)(2,1)S(1)}, u32[]{:S(2)}, u32[]{:S(2)}) async-start(bf16[16,48,128]{2,1,0:T(8,128)(2,1)} %broadcast_in_dim.20), calls=%async_computation.4 | async-start | bytes 393216 | tf_op jit(solution)/shard_map/all_to_all | solution.py:23
  86.7 4.6 %collective-permute-start.4 = (bf16[30,192]{1,0:T(8,128)(2,1)S(1)}, bf16[30,192]{1,0:T(8,128)(2,1)S(1)}, u32[]{:S(2)}, u32[]{:S(2)}) collective-permute-start(bf16[30,192]{1,0:T(8,128)(2,1)S(1)} %slice.747), channel_id=1, source_target_pairs={{8,0},{16,8},{24,16},{32,24},{40,32},{48,40},{56,48},{64,56},{72,6... | collective-permute-start | bytes 34568 | tf_op jit(solution)/shard_map/ppermute | solution.py:19
  91.6 1.9 %collective-permute-start.7 = (bf16[4,96,128]{2,1,0:T(8,128)(2,1)S(1)}, bf16[4,96,128]{2,1,0:T(8,128)(2,1)S(1)}, u32[]{:S(2)}, u32[]{:S(2)}) collective-permute-start(bf16[4,96,128]{2,1,0:T(8,128)(2,1)S(1)} %get-tuple-element.79), channel_id=1, source_target_pairs={{0,64},{32,96},{64,0},{96,32},{1,65},{33,97},{65,1},{97,33},{2,66}... | collective-permute-start | bytes 294920 | tf_op jit(solution)/shard_map/ppermute | solution.py:43
  93.5 3.9 %collective-permute-start.6 = (bf16[4,96,128]{2,1,0:T(8,128)(2,1)S(1)}, bf16[4,96,128]{2,1,0:T(8,128)(2,1)S(1)}, u32[]{:S(2)}, u32[]{:S(2)}) collective-permute-start(bf16[4,96,128]{2,1,0:T(8,128)(2,1)S(1)} %get-tuple-element.78), channel_id=1, source_target_pairs={{0,32},{32,0},{64,96},{96,64},{1,33},{33,1},{65,97},{97,65},{2,34}... | collective-permute-start | bytes 294920 | tf_op jit(solution)/shard_map/ppermute | solution.py:43
  97.5 3.4 %collective-permute-start.5 = (bf16[4,96,128]{2,1,0:T(8,128)(2,1)S(1)}, bf16[4,96,128]{2,1,0:T(8,128)(2,1)S(1)}, u32[]{:S(2)}, u32[]{:S(2)}) collective-permute-start(bf16[4,96,128]{2,1,0:T(8,128)(2,1)S(1)} %get-tuple-element.77), channel_id=1, source_target_pairs={{0,96},{32,64},{64,32},{96,0},{1,97},{33,65},{65,33},{97,1},{2,98}... | collective-permute-start | bytes 294920 | tf_op jit(solution)/shard_map/ppermute | solution.py:43
  100.9 4.1 %collective-permute-done.5 = bf16[4,96,128]{2,1,0:T(8,128)(2,1)S(1)} collective-permute-done((bf16[4,96,128]{2,1,0:T(8,128)(2,1)S(1)}, bf16[4,96,128]{2,1,0:T(8,128)(2,1)S(1)}, u32[]{:S(2)}, u32[]{:S(2)}) %collective-permute-start.5) | collective-permute-done | bytes 98336 | tf_op jit(solution)/shard_map/ppermute | solution.py:43
  105.1 0.7 pad_maximum_fusion.1
  105.8 7.6 %all-to-all-start.5 = ((bf16[4,144,128]{2,1,0:T(8,128)(2,1)}), bf16[4,144,128]{2,1,0:T(8,128)(2,1)S(1)}, u32[]{:S(2)}, u32[]{:S(2)}) async-start(bf16[4,144,128]{2,1,0:T(8,128)(2,1)} %pad_maximum_fusion.1), calls=%async_computation.5 | async-start | bytes 294912 | tf_op jit(solution)/shard_map/all_to_all | solution.py:23
  113.7 0.4 fusion.74
  114.2 0.7 copy.84
  114.9 0.7 copy.85
  115.6 12.9 %all-to-all-done.5 = bf16[4,144,128]{2,1,0:T(8,128)(2,1)S(1)} async-done(((bf16[4,144,128]{2,1,0:T(8,128)(2,1)}), bf16[4,144,128]{2,1,0:T(8,128)(2,1)S(1)}, u32[]{:S(2)}, u32[]{:S(2)}) %all-to-all-start.5) | async-done | bytes 147488 | tf_op jit(solution)/shard_map/all_to_all | solution.py:23
  128.6 0.6 maximum_maximum_fusion.3
  129.3 0.6 pad_maximum_fusion.7
  129.8 0.6 maximum_maximum_fusion.2
  (204 shorter events, 2.7 us)
Async XLA Ops:
  0.6 22.6 %copy-start = (bf16[128,4096]{1,0:T(8,128)(2,1)S(1)}, bf16[128,4096]{1,0:T(8,128)(2,1)}, u32[]{:S(2)}) copy-start(bf16[128,4096]{1,0:T(8,128)(2,1)} %param.8) | copy-start | bytes 3145732
  2.7 31.8 %collective-permute-start = (bf16[48,128]{0,1:T(8,128)(2,1)S(1)}, bf16[48,128]{0,1:T(8,128)(2,1)S(1)}, u32[]{:S(2)}, u32[]{:S(2)}) collective-permute-start(bf16[48,128]{0,1:T(8,128)(2,1)S(1)} %pad_maximum_fusion.6), channel_id=1, source_target_pairs={{0,8},{8,16},{16,24},{24,32},{32,40},{40,48},{48,56},{56,64},{64,7... | collective-permute-start | bytes 36872 | tf_op jit(solution)/shard_map/ppermute | solution.py:19
  8.5 37.5 %all-to-all-start = ((bf16[16,96,128]{2,1,0:T(8,128)(2,1)}), bf16[16,96,128]{2,1,0:T(8,128)(2,1)S(1)}, u32[]{:S(2)}, u32[]{:S(2)}) async-start(bf16[16,96,128]{2,1,0:T(8,128)(2,1)} %broadcast_in_dim.17), calls=%async_computation | async-start | bytes 786432 | tf_op jit(solution)/shard_map/all_to_all | solution.py:23
  24.0 10.1 %copy-start.1 = (f32[31,192]{1,0:T(8,128)S(1)}, f32[31,192]{1,0:T(8,128)}, u32[]{:S(2)}) copy-start(f32[31,192]{1,0:T(8,128)} %param.10) | copy-start | bytes 71428
  24.1 27.3 %collective-permute-start.2 = (bf16[128,1024]{0,1:T(8,128)(2,1)S(1)}, bf16[128,1024]{0,1:T(8,128)(2,1)S(1)}, u32[]{:S(2)}, u32[]{:S(2)}) collective-permute-start(bf16[128,1024]{0,1:T(8,128)(2,1)S(1)} %get-tuple-element.73), channel_id=1, source_target_pairs={{0,16},{8,24},{16,0},{24,8},{1,17},{9,25},{17,1},{25,9},{2,18},{10... | collective-permute-start | bytes 786440 | tf_op jit(solution)/shard_map/ppermute | solution.py:43
  29.0 22.8 %collective-permute-start.3 = (bf16[128,1024]{0,1:T(8,128)(2,1)S(1)}, bf16[128,1024]{0,1:T(8,128)(2,1)S(1)}, u32[]{:S(2)}, u32[]{:S(2)}) collective-permute-start(bf16[128,1024]{0,1:T(8,128)(2,1)S(1)} %get-tuple-element.71), channel_id=1, source_target_pairs={{0,8},{8,0},{16,24},{24,16},{1,9},{9,1},{17,25},{25,17},{2,10},{10... | collective-permute-start | bytes 786440 | tf_op jit(solution)/shard_map/ppermute | solution.py:43
  30.9 21.1 %collective-permute-start.1 = (bf16[128,1024]{0,1:T(8,128)(2,1)S(1)}, bf16[128,1024]{0,1:T(8,128)(2,1)S(1)}, u32[]{:S(2)}, u32[]{:S(2)}) collective-permute-start(bf16[128,1024]{0,1:T(8,128)(2,1)S(1)} %get-tuple-element.74), channel_id=1, source_target_pairs={{0,24},{8,16},{16,8},{24,0},{1,25},{9,17},{17,9},{25,1},{2,26},{10... | collective-permute-start | bytes 786440 | tf_op jit(solution)/shard_map/ppermute | solution.py:43
  34.2 0.8 copy-start.2
  34.2 0.8 copy-start.4
  34.2 0.8 copy-start.6
  34.2 0.8 copy-start.8
  46.8 9.6 %all-to-all-start.1 = ((f32[8,2,128]{2,1,0:T(2,128)}), f32[8,2,128]{2,1,0:T(2,128)S(1)}, u32[]{:S(2)}, u32[]{:S(2)}) async-start(f32[8,2,128]{2,1,0:T(2,128)} %broadcast_in_dim.18), calls=%async_computation.1 | async-start | bytes 16384 | tf_op jit(solution)/shard_map/all_to_all | solution.py:23
  51.7 4.7 %copy-start.56 = (f32[192]{0:T(256)S(1)}, f32[192]{0:T(256)}, u32[]{:S(2)}) copy-start(f32[192]{0:T(256)} %param.11) | copy-start | bytes 2308
  57.5 12.2 %all-to-all-start.2 = ((bf16[4,128,384]{2,1,0:T(8,128)(2,1)}), bf16[4,128,384]{2,1,0:T(8,128)(2,1)S(1)}, u32[]{:S(2)}, u32[]{:S(2)}) async-start(bf16[4,128,384]{2,1,0:T(8,128)(2,1)} %pad_maximum_fusion), calls=%async_computation.2 | async-start | bytes 786432 | tf_op jit(solution)/shard_map/all_to_all | solution.py:23
  70.6 8.6 %all-to-all-start.3 = ((f32[8,2,128]{2,1,0:T(2,128)}), f32[8,2,128]{2,1,0:T(2,128)S(1)}, u32[]{:S(2)}, u32[]{:S(2)}) async-start(f32[8,2,128]{2,1,0:T(2,128)} %broadcast_in_dim.19), calls=%async_computation.3 | async-start | bytes 16384 | tf_op jit(solution)/shard_map/all_to_all | solution.py:23
  81.3 23.8 %all-to-all-start.4 = ((bf16[16,48,128]{2,1,0:T(8,128)(2,1)}), bf16[16,48,128]{2,1,0:T(8,128)(2,1)S(1)}, u32[]{:S(2)}, u32[]{:S(2)}) async-start(bf16[16,48,128]{2,1,0:T(8,128)(2,1)} %broadcast_in_dim.20), calls=%async_computation.4 | async-start | bytes 393216 | tf_op jit(solution)/shard_map/all_to_all | solution.py:23
  86.7 14.1 %collective-permute-start.4 = (bf16[30,192]{1,0:T(8,128)(2,1)S(1)}, bf16[30,192]{1,0:T(8,128)(2,1)S(1)}, u32[]{:S(2)}, u32[]{:S(2)}) collective-permute-start(bf16[30,192]{1,0:T(8,128)(2,1)S(1)} %slice.747), channel_id=1, source_target_pairs={{8,0},{16,8},{24,16},{32,24},{40,32},{48,40},{56,48},{64,56},{72,6... | collective-permute-start | bytes 34568 | tf_op jit(solution)/shard_map/ppermute | solution.py:19
  91.3 22.1 %copy-start.3 = (f32[1,192]{1,0:T(1,128)S(1)}, f32[1,192]{1,0:T(1,128)}, u32[]{:S(2)}) copy-start(f32[1,192]{1,0:T(1,128)} %copy-done.2) | copy-start | bytes 2308
  91.3 22.1 %copy-start.5 = (f32[1,192]{1,0:T(1,128)S(1)}, f32[1,192]{1,0:T(1,128)}, u32[]{:S(2)}) copy-start(f32[1,192]{1,0:T(1,128)} %copy-done.4) | copy-start | bytes 2308
  91.3 22.1 %copy-start.7 = (f32[1,192]{1,0:T(1,128)S(1)}, f32[1,192]{1,0:T(1,128)}, u32[]{:S(2)}) copy-start(f32[1,192]{1,0:T(1,128)} %copy-done.6) | copy-start | bytes 2308
  91.3 22.1 %copy-start.9 = (f32[1,192]{1,0:T(1,128)S(1)}, f32[1,192]{1,0:T(1,128)}, u32[]{:S(2)}) copy-start(f32[1,192]{1,0:T(1,128)} %copy-done.8) | copy-start | bytes 2308
  91.3 22.1 %copy-start.11 = (f32[1,192]{1,0:T(1,128)S(1)}, f32[1,192]{1,0:T(1,128)}, u32[]{:S(2)}) copy-start(f32[1,192]{1,0:T(1,128)} %copy-done.10) | copy-start | bytes 2308
  91.3 22.1 %copy-start.13 = (f32[1,192]{1,0:T(1,128)S(1)}, f32[1,192]{1,0:T(1,128)}, u32[]{:S(2)}) copy-start(f32[1,192]{1,0:T(1,128)} %copy-done.12) | copy-start | bytes 2308
  91.3 22.1 %copy-start.15 = (f32[1,192]{1,0:T(1,128)S(1)}, f32[1,192]{1,0:T(1,128)}, u32[]{:S(2)}) copy-start(f32[1,192]{1,0:T(1,128)} %copy-done.14) | copy-start | bytes 2308
  91.4 22.1 %copy-start.17 = (f32[1,192]{1,0:T(1,128)S(1)}, f32[1,192]{1,0:T(1,128)}, u32[]{:S(2)}) copy-start(f32[1,192]{1,0:T(1,128)} %copy-done.16) | copy-start | bytes 2308
  91.4 22.1 %copy-start.19 = (f32[1,192]{1,0:T(1,128)S(1)}, f32[1,192]{1,0:T(1,128)}, u32[]{:S(2)}) copy-start(f32[1,192]{1,0:T(1,128)} %copy-done.18) | copy-start | bytes 2308
  91.4 22.1 %copy-start.21 = (f32[1,192]{1,0:T(1,128)S(1)}, f32[1,192]{1,0:T(1,128)}, u32[]{:S(2)}) copy-start(f32[1,192]{1,0:T(1,128)} %copy-done.20) | copy-start | bytes 2308
  91.4 22.1 %copy-start.23 = (f32[1,192]{1,0:T(1,128)S(1)}, f32[1,192]{1,0:T(1,128)}, u32[]{:S(2)}) copy-start(f32[1,192]{1,0:T(1,128)} %copy-done.22) | copy-start | bytes 2308
  91.4 22.1 %copy-start.25 = (f32[1,192]{1,0:T(1,128)S(1)}, f32[1,192]{1,0:T(1,128)}, u32[]{:S(2)}) copy-start(f32[1,192]{1,0:T(1,128)} %copy-done.24) | copy-start | bytes 2308
  91.4 22.1 %copy-start.27 = (f32[1,192]{1,0:T(1,128)S(1)}, f32[1,192]{1,0:T(1,128)}, u32[]{:S(2)}) copy-start(f32[1,192]{1,0:T(1,128)} %copy-done.26) | copy-start | bytes 2308
  91.4 22.1 %copy-start.29 = (f32[1,192]{1,0:T(1,128)S(1)}, f32[1,192]{1,0:T(1,128)}, u32[]{:S(2)}) copy-start(f32[1,192]{1,0:T(1,128)} %copy-done.28) | copy-start | bytes 2308
  91.4 22.1 %copy-start.31 = (f32[1,192]{1,0:T(1,128)S(1)}, f32[1,192]{1,0:T(1,128)}, u32[]{:S(2)}) copy-start(f32[1,192]{1,0:T(1,128)} %copy-done.30) | copy-start | bytes 2308
  91.4 22.1 %copy-start.33 = (f32[1,192]{1,0:T(1,128)S(1)}, f32[1,192]{1,0:T(1,128)}, u32[]{:S(2)}) copy-start(f32[1,192]{1,0:T(1,128)} %copy-done.32) | copy-start | bytes 2308
  91.4 22.1 %copy-start.35 = (f32[1,192]{1,0:T(1,128)S(1)}, f32[1,192]{1,0:T(1,128)}, u32[]{:S(2)}) copy-start(f32[1,192]{1,0:T(1,128)} %copy-done.34) | copy-start | bytes 2308
  91.5 22.1 %copy-start.37 = (f32[1,192]{1,0:T(1,128)S(1)}, f32[1,192]{1,0:T(1,128)}, u32[]{:S(2)}) copy-start(f32[1,192]{1,0:T(1,128)} %copy-done.36) | copy-start | bytes 2308
  91.5 22.1 %copy-start.39 = (f32[1,192]{1,0:T(1,128)S(1)}, f32[1,192]{1,0:T(1,128)}, u32[]{:S(2)}) copy-start(f32[1,192]{1,0:T(1,128)} %copy-done.38) | copy-start | bytes 2308
  91.5 22.1 %copy-start.41 = (f32[1,192]{1,0:T(1,128)S(1)}, f32[1,192]{1,0:T(1,128)}, u32[]{:S(2)}) copy-start(f32[1,192]{1,0:T(1,128)} %copy-done.40) | copy-start | bytes 2308
  91.5 22.1 %copy-start.43 = (f32[1,192]{1,0:T(1,128)S(1)}, f32[1,192]{1,0:T(1,128)}, u32[]{:S(2)}) copy-start(f32[1,192]{1,0:T(1,128)} %copy-done.42) | copy-start | bytes 2308
  91.5 22.1 %copy-start.45 = (f32[1,192]{1,0:T(1,128)S(1)}, f32[1,192]{1,0:T(1,128)}, u32[]{:S(2)}) copy-start(f32[1,192]{1,0:T(1,128)} %copy-done.44) | copy-start | bytes 2308
  91.5 22.1 %copy-start.47 = (f32[1,192]{1,0:T(1,128)S(1)}, f32[1,192]{1,0:T(1,128)}, u32[]{:S(2)}) copy-start(f32[1,192]{1,0:T(1,128)} %copy-done.46) | copy-start | bytes 2308
  91.5 22.1 %copy-start.49 = (f32[1,192]{1,0:T(1,128)S(1)}, f32[1,192]{1,0:T(1,128)}, u32[]{:S(2)}) copy-start(f32[1,192]{1,0:T(1,128)} %copy-done.48) | copy-start | bytes 2308
  91.5 22.1 %copy-start.51 = (f32[1,192]{1,0:T(1,128)S(1)}, f32[1,192]{1,0:T(1,128)}, u32[]{:S(2)}) copy-start(f32[1,192]{1,0:T(1,128)} %copy-done.50) | copy-start | bytes 2308
  91.5 22.1 %copy-start.53 = (f32[1,192]{1,0:T(1,128)S(1)}, f32[1,192]{1,0:T(1,128)}, u32[]{:S(2)}) copy-start(f32[1,192]{1,0:T(1,128)} %copy-done.52) | copy-start | bytes 2308
  91.5 22.1 %copy-start.55 = (f32[1,192]{1,0:T(1,128)S(1)}, f32[1,192]{1,0:T(1,128)}, u32[]{:S(2)}) copy-start(f32[1,192]{1,0:T(1,128)} %copy-done.54) | copy-start | bytes 2308
  91.6 9.3 %collective-permute-start.7 = (bf16[4,96,128]{2,1,0:T(8,128)(2,1)S(1)}, bf16[4,96,128]{2,1,0:T(8,128)(2,1)S(1)}, u32[]{:S(2)}, u32[]{:S(2)}) collective-permute-start(bf16[4,96,128]{2,1,0:T(8,128)(2,1)S(1)} %get-tuple-element.79), channel_id=1, source_target_pairs={{0,64},{32,96},{64,0},{96,32},{1,65},{33,97},{65,1},{97,33},{2,66}... | collective-permute-start | bytes 294920 | tf_op jit(solution)/shard_map/ppermute | solution.py:43
  93.5 7.4 %collective-permute-start.6 = (bf16[4,96,128]{2,1,0:T(8,128)(2,1)S(1)}, bf16[4,96,128]{2,1,0:T(8,128)(2,1)S(1)}, u32[]{:S(2)}, u32[]{:S(2)}) collective-permute-start(bf16[4,96,128]{2,1,0:T(8,128)(2,1)S(1)} %get-tuple-element.78), channel_id=1, source_target_pairs={{0,32},{32,0},{64,96},{96,64},{1,33},{33,1},{65,97},{97,65},{2,34}... | collective-permute-start | bytes 294920 | tf_op jit(solution)/shard_map/ppermute | solution.py:43
  97.5 7.6 %collective-permute-start.5 = (bf16[4,96,128]{2,1,0:T(8,128)(2,1)S(1)}, bf16[4,96,128]{2,1,0:T(8,128)(2,1)S(1)}, u32[]{:S(2)}, u32[]{:S(2)}) collective-permute-start(bf16[4,96,128]{2,1,0:T(8,128)(2,1)S(1)} %get-tuple-element.77), channel_id=1, source_target_pairs={{0,96},{32,64},{64,32},{96,0},{1,97},{33,65},{65,33},{97,1},{2,98}... | collective-permute-start | bytes 294920 | tf_op jit(solution)/shard_map/ppermute | solution.py:43
  105.8 22.7 %all-to-all-start.5 = ((bf16[4,144,128]{2,1,0:T(8,128)(2,1)}), bf16[4,144,128]{2,1,0:T(8,128)(2,1)S(1)}, u32[]{:S(2)}, u32[]{:S(2)}) async-start(bf16[4,144,128]{2,1,0:T(8,128)(2,1)} %pad_maximum_fusion.1), calls=%async_computation.5 | async-start | bytes 294912 | tf_op jit(solution)/shard_map/all_to_all | solution.py:23
  (23 other events, 18.7 us)

commit v2 on v1

--- a/solution.py
+++ b/solution.py
@@ -80,7 +80,8 @@
     y_here = lax.axis_index("sp_1")
     others = range(1, y_size)
 
-    weight = from_everyone(dense(out_weight), Z)
+    weight = with_layout_constraint(out_weight, Layout(major_to_minor=(1, 0)))
+    weight = from_everyone(dense(lax.optimization_barrier(weight)), Z)
     blocks = cotangent.reshape(rows_here, z_size, y_size, d_rows).transpose(2, 0, 1, 3)
     blocks = blocks.reshape(y_size, rows_here, z_size * d_rows)
     blocks = [lax.dynamic_index_in_dim(blocks, y_here ^ k, 0, False) for k in range(y_size)]
@@ -113,7 +114,10 @@
         jnp.dot(c, weight, preferred_element_type=jnp.float32).astype(jnp.bfloat16) for c in columns
     ]
     sent = [jnp.concatenate([part, swished], 1) for part in reordered(mix_parts, y_here)]
-    received = exchange(jnp.stack(sent), "sp_1")
+    near_here = lax.axis_index("z_near").astype(jnp.uint32)
+    near_at = [near_here ^ jnp.uint32(k) for k in range(lax.axis_size("z_near"))]
+    sent, near_at = lax.optimization_barrier((jnp.stack(sent), near_at))
+    received = exchange(sent, "sp_1")
     grad_mix = received[:, :, :width_dp].astype(jnp.float32).sum(axis=0)
     swished_y = reordered([received[i, :, width_dp:] for i in range(y_size)], y_here)
     weight_part = lax.dot_general(
@@ -124,9 +128,8 @@
     )
     weight_part = dense(weight_part.astype(jnp.bfloat16).reshape(z_size, d_rows, width_dp))
     near, far = (lax.axis_size("z_near"), lax.axis_size("z_far"))
-    near_here = lax.axis_index("z_near")
     part = weight_part.reshape(far, near, -1, weight_part.shape[-1])
-    part = [lax.dynamic_index_in_dim(part, near_here ^ k, 1, False) for k in range(near)]
+    part = [lax.dynamic_index_in_dim(part, near_at[k], 1, False) for k in range(near)]
     arrived = [swapped(part[near - 1], "z_near", near - 1)]
     arrived += [swapped(part[k], "z_near", k) for k in range(1, near - 1)]
 

time: 131 us -> 130 us (level)
  blocking collectives: 0 us -> 12 us
  waiting for transfers between devices: 44 us -> 35.9 us
  starting transfers between devices: 66.6 us -> 62.4 us
    all_to_all x0 -> x1, blocking collectives: none -> 12 us  [exchange(): return lax.all_to_all(blocks, axis, split_axis=0, concat_axis=0, tiled=True)]
    all_to_all x6 -> x5, waiting for transfers between devices: 39.9 us -> 31.8 us  [exchange(): return lax.all_to_all(blocks, axis, split_axis=0, concat_axis=0, tiled=True)]
    all_to_all x6 -> x5, starting transfers between devices: 39.4 us -> 35.2 us  [exchange(): return lax.all_to_all(blocks, axis, split_axis=0, concat_axis=0, tiled=True)]
    unnamed x119 -> x120, local copies, waits for them, and re-layouts: 4.25 us -> 5.12 us
  transfers between devices with their start and end apart: 14 -> 13, of which waited for: 6 -> 5; matrix products, arithmetic and copies ran while one was open for 7% -> 7% of each run, Pallas kernels for 0% -> 0%
where the time goes in v2:
time: 130 us; the launch traced here: 129 us
  starting transfers between devices  62.4 us (48%)
  waiting for transfers between devices  35.9 us (28%)
  blocking collectives  12 us (9%)
  local copies, waits for them, and re-layouts  9.31 us (7%)
  other arithmetic  5.65 us (4%)
  between operations  2.21 us (2%)
  matrix products  1.6 us (1%)
    all_to_all x5, starting transfers between devices, exchange(): return lax.all_to_all(blocks, axis, split_axis=0, concat_axis=0, tiled=True)  35.2 us
    all_to_all x5, waiting for transfers between devices, exchange(): return lax.all_to_all(blocks, axis, split_axis=0, concat_axis=0, tiled=True)  31.8 us
    ppermute x6, starting transfers between devices, swapped(): lax.ppermute(value, axis, [(i, i ^ k) for i in range(lax.axis_size(axis))])  19.2 us
    all_to_all x1, blocking collectives, exchange(): return lax.all_to_all(blocks, axis, split_axis=0, concat_axis=0, tiled=True)  12 us
    ppermute x2, starting transfers between devices, passed_along(): lax.ppermute(value, axis, [(source, source + steps) for source in range(f...  8.07 us
    unnamed x120, local copies, waits for them, and re-layouts  5.12 us
    ppermute x6, waiting for transfers between devices, swapped(): lax.ppermute(value, axis, [(i, i ^ k) for i in range(lax.axis_size(axis))])  4.14 us
    broadcast_in_dim x4, local copies, waits for them, and re-layouts, from_everyone(): jnp.broadcast_to(array, (lax.axis_size(axis), *array.shape))  2.71 us
  transfers between devices with their start and end apart: 13, of which 5 were waited for; matrix products, arithmetic and copies ran while one was open for 7% of the time, Pallas kernels for 0%

profile of v2, /device:TPU:64, one launch (start us, length us, event | category | flops | bytes accessed | tf_op | source)
XLA Modules:
  0.0 129.2 jit_solution(2083568177357305421)
XLA Ops:
  0.6 0.9 copy.82
  1.5 1.0 copy.83
  2.7 3.5 %collective-permute-start = (bf16[48,128]{0,1:T(8,128)(2,1)S(1)}, bf16[48,128]{0,1:T(8,128)(2,1)S(1)}, u32[]{:S(2)}, u32[]{:S(2)}) collective-permute-start(bf16[48,128]{0,1:T(8,128)(2,1)S(1)} %pad_maximum_fusion.6), channel_id=1, source_target_pairs={{0,8},{8,16},{16,24},{24,32},{32,40},{40,48},{48,56},{56,64},{64,7... | collective-permute-start | bytes 36872 | tf_op jit(solution)/shard_map/ppermute | solution.py:19
  6.2 0.9 copy.80
  7.3 0.8 broadcast_in_dim.17
  8.1 14.8 %all-to-all-start = ((bf16[16,96,128]{2,1,0:T(8,128)(2,1)}), bf16[16,96,128]{2,1,0:T(8,128)(2,1)S(1)}, u32[]{:S(2)}, u32[]{:S(2)}) async-start(bf16[16,96,128]{2,1,0:T(8,128)(2,1)} %broadcast_in_dim.17), calls=%async_computation | async-start | bytes 786432 | tf_op jit(solution)/shard_map/all_to_all | solution.py:23
  22.9 0.7 copy.85
  23.8 4.8 %collective-permute-start.2 = (bf16[128,1024]{0,1:T(8,128)(2,1)S(1)}, bf16[128,1024]{0,1:T(8,128)(2,1)S(1)}, u32[]{:S(2)}, u32[]{:S(2)}) collective-permute-start(bf16[128,1024]{0,1:T(8,128)(2,1)S(1)} %get-tuple-element.83), channel_id=1, source_target_pairs={{0,16},{8,24},{16,0},{24,8},{1,17},{9,25},{17,1},{25,9},{2,18},{10... | collective-permute-start | bytes 786440 | tf_op jit(solution)/shard_map/ppermute | solution.py:43
  28.6 2.0 %collective-permute-start.3 = (bf16[128,1024]{0,1:T(8,128)(2,1)S(1)}, bf16[128,1024]{0,1:T(8,128)(2,1)S(1)}, u32[]{:S(2)}, u32[]{:S(2)}) collective-permute-start(bf16[128,1024]{0,1:T(8,128)(2,1)S(1)} %get-tuple-element.81), channel_id=1, source_target_pairs={{0,8},{8,0},{16,24},{24,16},{1,9},{9,1},{17,25},{25,17},{2,10},{10... | collective-permute-start | bytes 786440 | tf_op jit(solution)/shard_map/ppermute | solution.py:43
  30.6 3.2 %collective-permute-start.1 = (bf16[128,1024]{0,1:T(8,128)(2,1)S(1)}, bf16[128,1024]{0,1:T(8,128)(2,1)S(1)}, u32[]{:S(2)}, u32[]{:S(2)}) collective-permute-start(bf16[128,1024]{0,1:T(8,128)(2,1)S(1)} %get-tuple-element.84), channel_id=1, source_target_pairs={{0,24},{8,16},{16,8},{24,0},{1,25},{9,17},{17,9},{25,1},{2,26},{10... | collective-permute-start | bytes 786440 | tf_op jit(solution)/shard_map/ppermute | solution.py:43
  34.3 0.4 add_convert_fusion
  35.1 10.6 %all-to-all-done = bf16[16,96,128]{2,1,0:T(8,128)(2,1)S(1)} async-done(((bf16[16,96,128]{2,1,0:T(8,128)(2,1)}), bf16[16,96,128]{2,1,0:T(8,128)(2,1)S(1)}, u32[]{:S(2)}, u32[]{:S(2)}) %all-to-all-start) | async-done | bytes 393248 | tf_op jit(solution)/shard_map/all_to_all | solution.py:23
  45.8 0.6 broadcast_in_dim.18
  46.4 4.3 %all-to-all-start.1 = ((f32[8,2,128]{2,1,0:T(2,128)}), f32[8,2,128]{2,1,0:T(2,128)S(1)}, u32[]{:S(2)}, u32[]{:S(2)}) async-start(f32[8,2,128]{2,1,0:T(2,128)} %broadcast_in_dim.18), calls=%async_computation.1 | async-start | bytes 16384 | tf_op jit(solution)/shard_map/all_to_all | solution.py:23
  50.8 0.3 convolution_convert_fusion.1
  51.1 0.3 convolution_convert_fusion.3
  51.4 0.3 convolution_convert_fusion.2
  51.7 0.3 broadcast_select_fusion.11
  52.0 4.0 %all-to-all-done.1 = f32[8,2,128]{2,1,0:T(2,128)S(1)} async-done(((f32[8,2,128]{2,1,0:T(2,128)}), f32[8,2,128]{2,1,0:T(2,128)S(1)}, u32[]{:S(2)}, u32[]{:S(2)}) %all-to-all-start.1) | async-done | bytes 8224 | tf_op jit(solution)/shard_map/all_to_all | solution.py:23
  56.1 0.1 fusion.34
  56.2 0.1 fusion.104
  56.4 12.0 %all_to_all.30 = bf16[4,128,384]{2,1,0:T(8,128)(2,1)S(1)} all-to-all(bf16[4,128,384]{2,1,0:T(8,128)(2,1)S(1)} %pad_maximum_fusion), channel_id=1, replica_groups=mesh['z_far'=4,'z_near'=4,'sp_1'=4,'dp'=8] {'sp_1'}, dimensions={0} | all-to-all | bytes 786432 | tf_op jit(solution)/shard_map/all_to_all | solution.py:23
  68.5 0.2 fusion.41
  68.7 0.6 broadcast_in_dim.19
  69.3 3.3 %all-to-all-start.3 = ((f32[8,2,128]{2,1,0:T(2,128)}), f32[8,2,128]{2,1,0:T(2,128)S(1)}, u32[]{:S(2)}, u32[]{:S(2)}) async-start(f32[8,2,128]{2,1,0:T(2,128)} %broadcast_in_dim.19), calls=%async_computation.3 | async-start | bytes 16384 | tf_op jit(solution)/shard_map/all_to_all | solution.py:23
  72.7 0.1 select_bitcast_fusion.3
  72.8 0.5 convolution_convert_fusion
  73.3 0.2 copy.92
  73.6 4.3 %all-to-all-done.3 = f32[8,2,128]{2,1,0:T(2,128)S(1)} async-done(((f32[8,2,128]{2,1,0:T(2,128)}), f32[8,2,128]{2,1,0:T(2,128)S(1)}, u32[]{:S(2)}, u32[]{:S(2)}) %all-to-all-start.3) | async-done | bytes 8224 | tf_op jit(solution)/shard_map/all_to_all | solution.py:23
  77.9 0.1 fusion.40
  78.1 0.3 fusion.57
  78.4 0.2 fusion.42
  79.3 0.7 broadcast_in_dim.20
  80.0 5.2 %all-to-all-start.4 = ((bf16[16,48,128]{2,1,0:T(8,128)(2,1)}), bf16[16,48,128]{2,1,0:T(8,128)(2,1)S(1)}, u32[]{:S(2)}, u32[]{:S(2)}) async-start(bf16[16,48,128]{2,1,0:T(8,128)(2,1)} %broadcast_in_dim.20), calls=%async_computation.4 | async-start | bytes 393216 | tf_op jit(solution)/shard_map/all_to_all | solution.py:23
  85.4 4.6 %collective-permute-start.4 = (bf16[30,192]{1,0:T(8,128)(2,1)S(1)}, bf16[30,192]{1,0:T(8,128)(2,1)S(1)}, u32[]{:S(2)}, u32[]{:S(2)}) collective-permute-start(bf16[30,192]{1,0:T(8,128)(2,1)S(1)} %slice.750), channel_id=1, source_target_pairs={{8,0},{16,8},{24,16},{32,24},{40,32},{48,40},{56,48},{64,56},{72,6... | collective-permute-start | bytes 34568 | tf_op jit(solution)/shard_map/ppermute | solution.py:19
  90.3 1.9 %collective-permute-start.7 = (bf16[4,96,128]{2,1,0:T(8,128)(2,1)S(1)}, bf16[4,96,128]{2,1,0:T(8,128)(2,1)S(1)}, u32[]{:S(2)}, u32[]{:S(2)}) collective-permute-start(bf16[4,96,128]{2,1,0:T(8,128)(2,1)S(1)} %get-tuple-element.89), channel_id=1, source_target_pairs={{0,64},{32,96},{64,0},{96,32},{1,65},{33,97},{65,1},{97,33},{2,66}... | collective-permute-start | bytes 294920 | tf_op jit(solution)/shard_map/ppermute | solution.py:43
  92.2 3.9 %collective-permute-start.6 = (bf16[4,96,128]{2,1,0:T(8,128)(2,1)S(1)}, bf16[4,96,128]{2,1,0:T(8,128)(2,1)S(1)}, u32[]{:S(2)}, u32[]{:S(2)}) collective-permute-start(bf16[4,96,128]{2,1,0:T(8,128)(2,1)S(1)} %get-tuple-element.88), channel_id=1, source_target_pairs={{0,32},{32,0},{64,96},{96,64},{1,33},{33,1},{65,97},{97,65},{2,34}... | collective-permute-start | bytes 294920 | tf_op jit(solution)/shard_map/ppermute | solution.py:43
  96.2 3.4 %collective-permute-start.5 = (bf16[4,96,128]{2,1,0:T(8,128)(2,1)S(1)}, bf16[4,96,128]{2,1,0:T(8,128)(2,1)S(1)}, u32[]{:S(2)}, u32[]{:S(2)}) collective-permute-start(bf16[4,96,128]{2,1,0:T(8,128)(2,1)S(1)} %get-tuple-element.87), channel_id=1, source_target_pairs={{0,96},{32,64},{64,32},{96,0},{1,97},{33,65},{65,33},{97,1},{2,98}... | collective-permute-start | bytes 294920 | tf_op jit(solution)/shard_map/ppermute | solution.py:43
  99.6 4.1 %collective-permute-done.5 = bf16[4,96,128]{2,1,0:T(8,128)(2,1)S(1)} collective-permute-done((bf16[4,96,128]{2,1,0:T(8,128)(2,1)S(1)}, bf16[4,96,128]{2,1,0:T(8,128)(2,1)S(1)}, u32[]{:S(2)}, u32[]{:S(2)}) %collective-permute-start.5) | collective-permute-done | bytes 98336 | tf_op jit(solution)/shard_map/ppermute | solution.py:43
  103.9 0.7 pad_maximum_fusion.1
  104.5 7.6 %all-to-all-start.5 = ((bf16[4,144,128]{2,1,0:T(8,128)(2,1)}), bf16[4,144,128]{2,1,0:T(8,128)(2,1)S(1)}, u32[]{:S(2)}, u32[]{:S(2)}) async-start(bf16[4,144,128]{2,1,0:T(8,128)(2,1)} %pad_maximum_fusion.1), calls=%async_computation.5 | async-start | bytes 294912 | tf_op jit(solution)/shard_map/all_to_all | solution.py:23
  112.4 0.4 fusion.74
  112.9 0.7 copy.97
  113.6 0.7 copy.98
  114.3 12.9 %all-to-all-done.5 = bf16[4,144,128]{2,1,0:T(8,128)(2,1)S(1)} async-done(((bf16[4,144,128]{2,1,0:T(8,128)(2,1)}), bf16[4,144,128]{2,1,0:T(8,128)(2,1)S(1)}, u32[]{:S(2)}, u32[]{:S(2)}) %all-to-all-start.5) | async-done | bytes 147488 | tf_op jit(solution)/shard_map/all_to_all | solution.py:23
  127.3 0.6 maximum_maximum_fusion.4
  128.0 0.6 pad_maximum_fusion.7
  128.5 0.6 maximum_maximum_fusion.2
  (205 shorter events, 2.6 us)
Async XLA Ops:
  1.5 21.4 %copy-start = (bf16[128,4096]{1,0:T(8,128)(2,1)S(1)}, bf16[128,4096]{1,0:T(8,128)(2,1)}, u32[]{:S(2)}) copy-start(bf16[128,4096]{1,0:T(8,128)(2,1)} %param.8) | copy-start | bytes 3145732
  2.7 31.4 %collective-permute-start = (bf16[48,128]{0,1:T(8,128)(2,1)S(1)}, bf16[48,128]{0,1:T(8,128)(2,1)S(1)}, u32[]{:S(2)}, u32[]{:S(2)}) collective-permute-start(bf16[48,128]{0,1:T(8,128)(2,1)S(1)} %pad_maximum_fusion.6), channel_id=1, source_target_pairs={{0,8},{8,16},{16,24},{24,32},{32,40},{40,48},{48,56},{56,64},{64,7... | collective-permute-start | bytes 36872 | tf_op jit(solution)/shard_map/ppermute | solution.py:19
  8.1 37.5 %all-to-all-start = ((bf16[16,96,128]{2,1,0:T(8,128)(2,1)}), bf16[16,96,128]{2,1,0:T(8,128)(2,1)S(1)}, u32[]{:S(2)}, u32[]{:S(2)}) async-start(bf16[16,96,128]{2,1,0:T(8,128)(2,1)} %broadcast_in_dim.17), calls=%async_computation | async-start | bytes 786432 | tf_op jit(solution)/shard_map/all_to_all | solution.py:23
  23.7 10.1 %copy-start.1 = (f32[31,192]{1,0:T(8,128)S(1)}, f32[31,192]{1,0:T(8,128)}, u32[]{:S(2)}) copy-start(f32[31,192]{1,0:T(8,128)} %param.10) | copy-start | bytes 71428
  23.8 27.3 %collective-permute-start.2 = (bf16[128,1024]{0,1:T(8,128)(2,1)S(1)}, bf16[128,1024]{0,1:T(8,128)(2,1)S(1)}, u32[]{:S(2)}, u32[]{:S(2)}) collective-permute-start(bf16[128,1024]{0,1:T(8,128)(2,1)S(1)} %get-tuple-element.83), channel_id=1, source_target_pairs={{0,16},{8,24},{16,0},{24,8},{1,17},{9,25},{17,1},{25,9},{2,18},{10... | collective-permute-start | bytes 786440 | tf_op jit(solution)/shard_map/ppermute | solution.py:43
  28.6 22.8 %collective-permute-start.3 = (bf16[128,1024]{0,1:T(8,128)(2,1)S(1)}, bf16[128,1024]{0,1:T(8,128)(2,1)S(1)}, u32[]{:S(2)}, u32[]{:S(2)}) collective-permute-start(bf16[128,1024]{0,1:T(8,128)(2,1)S(1)} %get-tuple-element.81), channel_id=1, source_target_pairs={{0,8},{8,0},{16,24},{24,16},{1,9},{9,1},{17,25},{25,17},{2,10},{10... | collective-permute-start | bytes 786440 | tf_op jit(solution)/shard_map/ppermute | solution.py:43
  30.6 21.1 %collective-permute-start.1 = (bf16[128,1024]{0,1:T(8,128)(2,1)S(1)}, bf16[128,1024]{0,1:T(8,128)(2,1)S(1)}, u32[]{:S(2)}, u32[]{:S(2)}) collective-permute-start(bf16[128,1024]{0,1:T(8,128)(2,1)S(1)} %get-tuple-element.84), channel_id=1, source_target_pairs={{0,24},{8,16},{16,8},{24,0},{1,25},{9,17},{17,9},{25,1},{2,26},{10... | collective-permute-start | bytes 786440 | tf_op jit(solution)/shard_map/ppermute | solution.py:43
  33.8 0.8 copy-start.2
  33.8 0.8 copy-start.4
  33.9 0.8 copy-start.6
  33.9 0.8 copy-start.8
  33.9 0.8 copy-start.10
  46.4 9.6 %all-to-all-start.1 = ((f32[8,2,128]{2,1,0:T(2,128)}), f32[8,2,128]{2,1,0:T(2,128)S(1)}, u32[]{:S(2)}, u32[]{:S(2)}) async-start(f32[8,2,128]{2,1,0:T(2,128)} %broadcast_in_dim.18), calls=%async_computation.1 | async-start | bytes 16384 | tf_op jit(solution)/shard_map/all_to_all | solution.py:23
  51.4 4.7 %copy-start.56 = (f32[192]{0:T(256)S(1)}, f32[192]{0:T(256)}, u32[]{:S(2)}) copy-start(f32[192]{0:T(256)} %param.11) | copy-start | bytes 2308
  69.3 8.6 %all-to-all-start.3 = ((f32[8,2,128]{2,1,0:T(2,128)}), f32[8,2,128]{2,1,0:T(2,128)S(1)}, u32[]{:S(2)}, u32[]{:S(2)}) async-start(f32[8,2,128]{2,1,0:T(2,128)} %broadcast_in_dim.19), calls=%async_computation.3 | async-start | bytes 16384 | tf_op jit(solution)/shard_map/all_to_all | solution.py:23
  80.0 23.7 %all-to-all-start.4 = ((bf16[16,48,128]{2,1,0:T(8,128)(2,1)}), bf16[16,48,128]{2,1,0:T(8,128)(2,1)S(1)}, u32[]{:S(2)}, u32[]{:S(2)}) async-start(bf16[16,48,128]{2,1,0:T(8,128)(2,1)} %broadcast_in_dim.20), calls=%async_computation.4 | async-start | bytes 393216 | tf_op jit(solution)/shard_map/all_to_all | solution.py:23
  85.4 14.1 %collective-permute-start.4 = (bf16[30,192]{1,0:T(8,128)(2,1)S(1)}, bf16[30,192]{1,0:T(8,128)(2,1)S(1)}, u32[]{:S(2)}, u32[]{:S(2)}) collective-permute-start(bf16[30,192]{1,0:T(8,128)(2,1)S(1)} %slice.750), channel_id=1, source_target_pairs={{8,0},{16,8},{24,16},{32,24},{40,32},{48,40},{56,48},{64,56},{72,6... | collective-permute-start | bytes 34568 | tf_op jit(solution)/shard_map/ppermute | solution.py:19
  90.0 22.1 %copy-start.3 = (f32[1,192]{1,0:T(1,128)S(1)}, f32[1,192]{1,0:T(1,128)}, u32[]{:S(2)}) copy-start(f32[1,192]{1,0:T(1,128)} %copy-done.2) | copy-start | bytes 2308
  90.0 22.1 %copy-start.5 = (f32[1,192]{1,0:T(1,128)S(1)}, f32[1,192]{1,0:T(1,128)}, u32[]{:S(2)}) copy-start(f32[1,192]{1,0:T(1,128)} %copy-done.4) | copy-start | bytes 2308
  90.0 22.1 %copy-start.7 = (f32[1,192]{1,0:T(1,128)S(1)}, f32[1,192]{1,0:T(1,128)}, u32[]{:S(2)}) copy-start(f32[1,192]{1,0:T(1,128)} %copy-done.6) | copy-start | bytes 2308
  90.0 22.1 %copy-start.9 = (f32[1,192]{1,0:T(1,128)S(1)}, f32[1,192]{1,0:T(1,128)}, u32[]{:S(2)}) copy-start(f32[1,192]{1,0:T(1,128)} %copy-done.8) | copy-start | bytes 2308
  90.0 22.1 %copy-start.11 = (f32[1,192]{1,0:T(1,128)S(1)}, f32[1,192]{1,0:T(1,128)}, u32[]{:S(2)}) copy-start(f32[1,192]{1,0:T(1,128)} %copy-done.10) | copy-start | bytes 2308
  90.0 22.1 %copy-start.13 = (f32[1,192]{1,0:T(1,128)S(1)}, f32[1,192]{1,0:T(1,128)}, u32[]{:S(2)}) copy-start(f32[1,192]{1,0:T(1,128)} %copy-done.12) | copy-start | bytes 2308
  90.1 22.1 %copy-start.15 = (f32[1,192]{1,0:T(1,128)S(1)}, f32[1,192]{1,0:T(1,128)}, u32[]{:S(2)}) copy-start(f32[1,192]{1,0:T(1,128)} %copy-done.14) | copy-start | bytes 2308
  90.1 22.1 %copy-start.17 = (f32[1,192]{1,0:T(1,128)S(1)}, f32[1,192]{1,0:T(1,128)}, u32[]{:S(2)}) copy-start(f32[1,192]{1,0:T(1,128)} %copy-done.16) | copy-start | bytes 2308
  90.1 22.1 %copy-start.19 = (f32[1,192]{1,0:T(1,128)S(1)}, f32[1,192]{1,0:T(1,128)}, u32[]{:S(2)}) copy-start(f32[1,192]{1,0:T(1,128)} %copy-done.18) | copy-start | bytes 2308
  90.1 22.1 %copy-start.21 = (f32[1,192]{1,0:T(1,128)S(1)}, f32[1,192]{1,0:T(1,128)}, u32[]{:S(2)}) copy-start(f32[1,192]{1,0:T(1,128)} %copy-done.20) | copy-start | bytes 2308
  90.1 22.1 %copy-start.23 = (f32[1,192]{1,0:T(1,128)S(1)}, f32[1,192]{1,0:T(1,128)}, u32[]{:S(2)}) copy-start(f32[1,192]{1,0:T(1,128)} %copy-done.22) | copy-start | bytes 2308
  90.1 22.1 %copy-start.25 = (f32[1,192]{1,0:T(1,128)S(1)}, f32[1,192]{1,0:T(1,128)}, u32[]{:S(2)}) copy-start(f32[1,192]{1,0:T(1,128)} %copy-done.24) | copy-start | bytes 2308
  90.1 22.1 %copy-start.27 = (f32[1,192]{1,0:T(1,128)S(1)}, f32[1,192]{1,0:T(1,128)}, u32[]{:S(2)}) copy-start(f32[1,192]{1,0:T(1,128)} %copy-done.26) | copy-start | bytes 2308
  90.1 22.1 %copy-start.29 = (f32[1,192]{1,0:T(1,128)S(1)}, f32[1,192]{1,0:T(1,128)}, u32[]{:S(2)}) copy-start(f32[1,192]{1,0:T(1,128)} %copy-done.28) | copy-start | bytes 2308
  90.1 22.1 %copy-start.31 = (f32[1,192]{1,0:T(1,128)S(1)}, f32[1,192]{1,0:T(1,128)}, u32[]{:S(2)}) copy-start(f32[1,192]{1,0:T(1,128)} %copy-done.30) | copy-start | bytes 2308
  90.1 22.1 %copy-start.33 = (f32[1,192]{1,0:T(1,128)S(1)}, f32[1,192]{1,0:T(1,128)}, u32[]{:S(2)}) copy-start(f32[1,192]{1,0:T(1,128)} %copy-done.32) | copy-start | bytes 2308
  90.2 22.1 %copy-start.35 = (f32[1,192]{1,0:T(1,128)S(1)}, f32[1,192]{1,0:T(1,128)}, u32[]{:S(2)}) copy-start(f32[1,192]{1,0:T(1,128)} %copy-done.34) | copy-start | bytes 2308
  90.2 22.1 %copy-start.37 = (f32[1,192]{1,0:T(1,128)S(1)}, f32[1,192]{1,0:T(1,128)}, u32[]{:S(2)}) copy-start(f32[1,192]{1,0:T(1,128)} %copy-done.36) | copy-start | bytes 2308
  90.2 22.1 %copy-start.39 = (f32[1,192]{1,0:T(1,128)S(1)}, f32[1,192]{1,0:T(1,128)}, u32[]{:S(2)}) copy-start(f32[1,192]{1,0:T(1,128)} %copy-done.38) | copy-start | bytes 2308
  90.2 22.1 %copy-start.41 = (f32[1,192]{1,0:T(1,128)S(1)}, f32[1,192]{1,0:T(1,128)}, u32[]{:S(2)}) copy-start(f32[1,192]{1,0:T(1,128)} %copy-done.40) | copy-start | bytes 2308
  90.2 22.1 %copy-start.43 = (f32[1,192]{1,0:T(1,128)S(1)}, f32[1,192]{1,0:T(1,128)}, u32[]{:S(2)}) copy-start(f32[1,192]{1,0:T(1,128)} %copy-done.42) | copy-start | bytes 2308
  90.2 22.1 %copy-start.45 = (f32[1,192]{1,0:T(1,128)S(1)}, f32[1,192]{1,0:T(1,128)}, u32[]{:S(2)}) copy-start(f32[1,192]{1,0:T(1,128)} %copy-done.44) | copy-start | bytes 2308
  90.2 22.1 %copy-start.47 = (f32[1,192]{1,0:T(1,128)S(1)}, f32[1,192]{1,0:T(1,128)}, u32[]{:S(2)}) copy-start(f32[1,192]{1,0:T(1,128)} %copy-done.46) | copy-start | bytes 2308
  90.2 22.1 %copy-start.49 = (f32[1,192]{1,0:T(1,128)S(1)}, f32[1,192]{1,0:T(1,128)}, u32[]{:S(2)}) copy-start(f32[1,192]{1,0:T(1,128)} %copy-done.48) | copy-start | bytes 2308
  90.2 22.1 %copy-start.51 = (f32[1,192]{1,0:T(1,128)S(1)}, f32[1,192]{1,0:T(1,128)}, u32[]{:S(2)}) copy-start(f32[1,192]{1,0:T(1,128)} %copy-done.50) | copy-start | bytes 2308
  90.2 22.1 %copy-start.53 = (f32[1,192]{1,0:T(1,128)S(1)}, f32[1,192]{1,0:T(1,128)}, u32[]{:S(2)}) copy-start(f32[1,192]{1,0:T(1,128)} %copy-done.52) | copy-start | bytes 2308
  90.3 22.1 %copy-start.55 = (f32[1,192]{1,0:T(1,128)S(1)}, f32[1,192]{1,0:T(1,128)}, u32[]{:S(2)}) copy-start(f32[1,192]{1,0:T(1,128)} %copy-done.54) | copy-start | bytes 2308
  90.3 9.3 %collective-permute-start.7 = (bf16[4,96,128]{2,1,0:T(8,128)(2,1)S(1)}, bf16[4,96,128]{2,1,0:T(8,128)(2,1)S(1)}, u32[]{:S(2)}, u32[]{:S(2)}) collective-permute-start(bf16[4,96,128]{2,1,0:T(8,128)(2,1)S(1)} %get-tuple-element.89), channel_id=1, source_target_pairs={{0,64},{32,96},{64,0},{96,32},{1,65},{33,97},{65,1},{97,33},{2,66}... | collective-permute-start | bytes 294920 | tf_op jit(solution)/shard_map/ppermute | solution.py:43
  92.2 7.4 %collective-permute-start.6 = (bf16[4,96,128]{2,1,0:T(8,128)(2,1)S(1)}, bf16[4,96,128]{2,1,0:T(8,128)(2,1)S(1)}, u32[]{:S(2)}, u32[]{:S(2)}) collective-permute-start(bf16[4,96,128]{2,1,0:T(8,128)(2,1)S(1)} %get-tuple-element.88), channel_id=1, source_target_pairs={{0,32},{32,0},{64,96},{96,64},{1,33},{33,1},{65,97},{97,65},{2,34}... | collective-permute-start | bytes 294920 | tf_op jit(solution)/shard_map/ppermute | solution.py:43
  96.2 7.6 %collective-permute-start.5 = (bf16[4,96,128]{2,1,0:T(8,128)(2,1)S(1)}, bf16[4,96,128]{2,1,0:T(8,128)(2,1)S(1)}, u32[]{:S(2)}, u32[]{:S(2)}) collective-permute-start(bf16[4,96,128]{2,1,0:T(8,128)(2,1)S(1)} %get-tuple-element.87), channel_id=1, source_target_pairs={{0,96},{32,64},{64,32},{96,0},{1,97},{33,65},{65,33},{97,1},{2,98}... | collective-permute-start | bytes 294920 | tf_op jit(solution)/shard_map/ppermute | solution.py:43
  104.5 22.7 %all-to-all-start.5 = ((bf16[4,144,128]{2,1,0:T(8,128)(2,1)}), bf16[4,144,128]{2,1,0:T(8,128)(2,1)S(1)}, u32[]{:S(2)}, u32[]{:S(2)}) async-start(bf16[4,144,128]{2,1,0:T(8,128)(2,1)} %pad_maximum_fusion.1), calls=%async_computation.5 | async-start | bytes 294912 | tf_op jit(solution)/shard_map/all_to_all | solution.py:23
  (22 other events, 18.0 us)
